TPU v7x, 32 devices: a whole 2x2x4 slice. The times are simulated.
32 devices in a mesh: sp: 16 (over z, y, x), tp: 2 (over core).
Axes of the slice: x: 2, y: 2, z: 4, core: 2. Of those that a mesh axis runs over, the one named last changes fastest.
Arguments:
- stream_mid: bfloat16 [3072, 2048], P('sp'), may hold values from -6 to 6
- d_out: bfloat16 [3072, 2048], P('sp'), may hold values from -6 to 6
- route_ids: int32 [3072, 2], P('sp'), may hold values from 0 to 15, all different within a row; in each aligned block of 192 rows (0 to 191, 192 to 383, ...) at most 48 rows name the same one
- route_weights: float32 [3072, 2], P('sp'), may hold values from 0.3 to 1.5
- gate_pre: bfloat16 [3072, 2048], P('sp', 'tp'), may hold values from -6 to 6
- lru_out: bfloat16 [3072, 2048], P('sp', 'tp'), may hold values from -6 to 6
- log_decay: float32 [3072, 2048], P('sp', 'tp'), may hold values from -2.5 to 0
- w_out: bfloat16 [2048, 2048], P('tp'), may hold values from -0.125 to 0.125
- exp_gate: bfloat16 [16, 2048, 1024], P('sp', None, 'tp'), may hold values from -0.125 to 0.125
- exp_up: bfloat16 [16, 2048, 1024], P('sp', None, 'tp'), may hold values from -0.125 to 0.125
- exp_down: bfloat16 [16, 1024, 2048], P('sp', 'tp'), may hold values from -0.1875 to 0.1875
Outputs:
- grad_exp_gate: float32 [16, 2048, 1024], P('sp', None, 'tp')
- grad_exp_up: float32 [16, 2048, 1024], P('sp', None, 'tp')
- grad_exp_down: float32 [16, 1024, 2048], P('sp', 'tp')
- grad_out_proj: float32 [2048, 2048], P('sp', 'tp')
- d_gate: bfloat16 [3072, 2048], P('sp', 'tp')
- d_drive: float32 [3072, 2048], P('sp', 'tp')
- d_log_decay: float32 [3072, 2048], P('sp', 'tp')
Inputs may be any that keep to these rules, and one draw needn't show every extreme that they name: `route_ids`: each row names 2 different experts; among the rows of one index of sp no expert is named by more than 48 rows, and in every draw some expert is named by exactly 48 of them.
All inputs are finite; a program needn't handle non-finite values.
Results may differ from a plain program's by a relative error of at most 0.0069.
Values may be sent and summed in bfloat16 or wider, within the bound.
A program may use at most 128 MiB of HBM per device.

v0:
```python
import jax
import jax.numpy as jnp
from jax import lax
from jax.sharding import PartitionSpec as P

TOPK = 2
EXP_DEV = 1


def entering(value, axis, join, neutral):
    count, mine = (lax.axis_size(axis), lax.axis_index(axis))
    pieces = jax.tree.map(lambda part: lax.all_gather(part, axis), value)
    pieces = jax.tree.map(lambda part: part[::-1], pieces)
    mine = count - 1 - mine
    subtotal = jax.tree.map(
        lambda part, zero: jnp.full_like(part, 0) + jnp.asarray(zero, part.dtype), value, neutral
    )

    def turn(position, subtotal):
        longer = join(subtotal, jax.tree.map(lambda part: part[position], pieces))
        return jax.tree.map(lambda new, old: jnp.where(position < mine, new, old), longer, subtotal)

    return lax.fori_loop(0, count - 1, turn, subtotal)


def shifted(value, axis, steps):
    count = lax.axis_size(axis)
    leading, last = (max(0, -steps), min(count, count - steps))
    return lax.ppermute(value, axis, [(source, source + steps) for source in range(leading, last)])


def contract_rows(left, right):
    return lax.dot_general(
        left, right, (((0,), (0,)), ((), ())), preferred_element_type=jnp.float32
    )


def contract_cols(left, right):
    return lax.dot_general(
        left, right, (((1,), (1,)), ((), ())), preferred_element_type=jnp.float32
    )


def local_recurrence(decay_rate, drive):
    coeffs = jnp.concatenate([decay_rate[1:], jnp.zeros_like(decay_rate[:1])], axis=0)

    def combine(earlier, later):
        return (earlier[0] * later[0], later[0] * earlier[1] + later[1])

    _, carried = lax.associative_scan(combine, (jnp.flip(coeffs, 0), jnp.flip(drive, 0)), axis=0)
    return jnp.flip(carried, 0)


def link_blocks(earlier, later):
    return (earlier[0] * later[0], later[0] * earlier[1] + later[1])


def on_device(
    stream_mid,
    d_out,
    route_ids,
    route_weights,
    gate_pre,
    lru_out,
    log_decay,
    w_out,
    exp_gate,
    exp_up,
    exp_down,
):
    rows_local = d_out.shape[0]
    model_width = d_out.shape[1]
    sp_count = lax.axis_size("sp")
    tp_count = lax.axis_size("tp")
    expert_count = EXP_DEV * sp_count
    capacity = max(2, 2 * rows_local * TOPK // expert_count)
    slot_count = expert_count * capacity
    flat_ids = route_ids.reshape(-1)
    onehot = (flat_ids[:, None] == jnp.arange(expert_count, dtype=jnp.int32)[None, :]).astype(
        jnp.int32
    )
    slot_rank = jnp.sum((jnp.cumsum(onehot, axis=0) - 1) * onehot, axis=1)
    slot_index = flat_ids * capacity + slot_rank
    token_owner = jnp.arange(rows_local * TOPK, dtype=jnp.int32) // TOPK
    source = jnp.full((slot_count,), rows_local, jnp.int32).at[slot_index].set(token_owner)
    slot_weight = (
        jnp.zeros((slot_count,), jnp.float32).at[slot_index].set(route_weights.reshape(-1))
    )
    padded_stream = jnp.concatenate([stream_mid, jnp.zeros((1, model_width), jnp.bfloat16)], axis=0)
    padded_cot = jnp.concatenate([d_out, jnp.zeros((1, model_width), jnp.bfloat16)], axis=0)
    sent_rows = padded_stream[source].reshape(sp_count, EXP_DEV * capacity, model_width)
    sent_cot = (slot_weight[:, None] * padded_cot[source].astype(jnp.float32)).astype(jnp.bfloat16)
    sent_cot = sent_cot.reshape(sp_count, EXP_DEV * capacity, model_width)
    half_cols = model_width // tp_count
    column_start = lax.axis_index("tp") * half_cols
    rows_piece = lax.dynamic_slice_in_dim(sent_rows, column_start, half_cols, 2)
    cot_piece = lax.dynamic_slice_in_dim(sent_cot, column_start, half_cols, 2)
    got_rows, got_cot = (
        lax.all_to_all(rows_piece, "sp", split_axis=0, concat_axis=0, tiled=True),
        lax.all_to_all(cot_piece, "sp", split_axis=0, concat_axis=0, tiled=True),
    )
    arrived_rows, arrived_cot = (
        lax.all_gather(got_rows, "tp", axis=2, tiled=True),
        lax.all_gather(got_cot, "tp", axis=2, tiled=True),
    )
    expert_rows = arrived_rows.reshape(sp_count, EXP_DEV, capacity, model_width).transpose(
        1, 0, 2, 3
    )
    expert_rows = expert_rows.reshape(EXP_DEV, sp_count * capacity, model_width)
    expert_cot = arrived_cot.reshape(sp_count, EXP_DEV, capacity, model_width).transpose(1, 0, 2, 3)
    expert_cot = expert_cot.reshape(EXP_DEV, sp_count * capacity, model_width)
    inputs = expert_rows[0]
    cotangent = expert_cot[0]
    gate_proj = jnp.dot(inputs, exp_gate[0], preferred_element_type=jnp.float32)
    up_proj = jnp.dot(inputs, exp_up[0], preferred_element_type=jnp.float32)
    gate_sigmoid = jax.nn.sigmoid(gate_proj)
    gate_act = gate_proj * gate_sigmoid
    hidden = (gate_act * up_proj).astype(jnp.bfloat16)
    back_hidden = contract_cols(cotangent, exp_down[0])
    grad_gate_pre = (
        back_hidden * up_proj * gate_sigmoid * (1.0 + gate_proj * (1.0 - gate_sigmoid))
    ).astype(jnp.bfloat16)
    grad_up_pre = (back_hidden * gate_act).astype(jnp.bfloat16)
    down_grads = [contract_rows(hidden, cotangent)]
    gate_grads = [contract_rows(inputs, grad_gate_pre)]
    up_grads = [contract_rows(inputs, grad_up_pre)]
    back_terms = [contract_cols(grad_gate_pre, exp_gate[0]) + contract_cols(grad_up_pre, exp_up[0])]
    back_stack = jnp.stack(back_terms, axis=0).reshape(EXP_DEV, sp_count, capacity, model_width)
    back_stack = back_stack.transpose(1, 0, 2, 3).reshape(sp_count, EXP_DEV * capacity, model_width)
    back_stack = back_stack.astype(jnp.bfloat16)
    summed_back = lax.psum(back_stack, "tp").astype(jnp.float32).astype(jnp.bfloat16)
    returned = lax.all_to_all(summed_back, "sp", split_axis=0, concat_axis=0, tiled=True)
    returned = returned.reshape(slot_count, model_width)
    routed_back = jnp.sum(
        returned[slot_index].astype(jnp.float32).reshape(rows_local, TOPK, model_width), axis=1
    )
    d_mid = (d_out.astype(jnp.float32) + routed_back).astype(jnp.bfloat16)
    d_gated = contract_cols(d_mid, w_out)
    state_vals = lru_out.astype(jnp.float32)
    gelu_val, gelu_back = jax.vjp(jax.nn.gelu, gate_pre.astype(jnp.float32))
    gated = (gelu_val * state_vals).astype(jnp.bfloat16)
    grad_out_proj = lax.psum_scatter(
        contract_rows(d_mid, gated), "sp", scatter_dimension=0, tiled=True
    )
    d_gate = gelu_back(d_gated * state_vals)[0].astype(jnp.bfloat16)
    decay_rate = jnp.exp(log_decay)
    local_grad = local_recurrence(decay_rate, d_gated * gelu_val)
    block_decay = jnp.exp(jnp.sum(log_decay, axis=0))
    head_term = decay_rate[0] * local_grad[0]
    channel_ones = jnp.ones_like(block_decay)
    channel_zeros = jnp.zeros_like(head_term)
    _, incoming = entering(
        (block_decay, head_term), "sp", link_blocks, (channel_ones, channel_zeros)
    )
    suffix_log = jnp.flip(jnp.cumsum(jnp.flip(log_decay, 0), axis=0), 0) - log_decay
    d_drive = local_grad + jnp.exp(suffix_log) * incoming[None, :]
    before_row = shifted(lru_out[-1:], "sp", 1)
    prev_state = jnp.concatenate([before_row.astype(jnp.float32), state_vals[:-1]], axis=0)
    d_log_decay = d_drive * decay_rate * prev_state
    return (
        jnp.stack(gate_grads, axis=0),
        jnp.stack(up_grads, axis=0),
        jnp.stack(down_grads, axis=0),
        grad_out_proj,
        d_gate,
        d_drive,
        d_log_decay,
    )


def solution(mesh):
    in_specs = (
        P("sp", None),
        P("sp", None),
        P("sp", None),
        P("sp", None),
        P("sp", "tp"),
        P("sp", "tp"),
        P("sp", "tp"),
        P("tp", None),
        P("sp", None, "tp"),
        P("sp", None, "tp"),
        P("sp", "tp", None),
    )
    out_specs = (
        P("sp", None, "tp"),
        P("sp", None, "tp"),
        P("sp", "tp", None),
        P("sp", "tp"),
        P("sp", "tp"),
        P("sp", "tp"),
        P("sp", "tp"),
    )
    return jax.shard_map(
        on_device, mesh=mesh, in_specs=in_specs, out_specs=out_specs, check_vma=False
    )
```

profile of v0, /device:TPU:0, one launch (start us, length us, event | category | flops | bytes accessed | tf_op | source)
XLA Modules:
  0.0 441.6 jit_solution(6955857391817476772)
XLA Ops:
  7.2 0.9 copy.28
  9.1 0.9 reduce-window.14
  10.6 2.9 scatter_custom_fusion
  13.6 1.2 concatenate.33
  14.8 4.2 gather_fusion
  19.0 2.7 constant_dynamic-slice_fusion.2
  21.8 8.4 %all-to-all-start = ((bf16[16,48,1024]{2,1,0:T(8,128)(2,1)}), bf16[16,48,1024]{2,1,0:T(8,128)(2,1)}, u32[]{:S(2)}, u32[]{:S(2)}) async-start(bf16[16,48,1024]{2,1,0:T(8,128)(2,1)} %constant_dynamic-slice_fusion.2), calls=%async_computation | async-start | bytes 3145728 | tf_op jit(solution)/shard_map/all_to_all | solution.py:99
  30.2 1.2 concatenate.34
  31.4 4.2 gather_fusion.1
  35.9 2.9 scatter_custom_fusion.1
  38.9 25.4 %all-to-all-done = bf16[16,48,1024]{2,1,0:T(8,128)(2,1)} async-done(((bf16[16,48,1024]{2,1,0:T(8,128)(2,1)}), bf16[16,48,1024]{2,1,0:T(8,128)(2,1)}, u32[]{:S(2)}, u32[]{:S(2)}) %all-to-all-start) | async-done | bytes 1572896 | tf_op jit(solution)/shard_map/all_to_all | solution.py:99
  64.4 1.7 fusion
  66.1 44.5 %all_to_all.15 = bf16[16,48,1024]{2,1,0:T(8,128)(2,1)} all-to-all(bf16[16,48,1024]{2,1,0:T(8,128)(2,1)S(1)} %fusion), channel_id=1, replica_groups=mesh['sp'=16,'tp'=2] {'sp'}, dimensions={0} | all-to-all | bytes 3145728 | tf_op jit(solution)/shard_map/all_to_all | solution.py:100
  111.0 5.0 %fusion.3 = f32[768,512]{1,0:T(8,128)} fusion(bf16[768,2048]{1,0:T(8,128)(2,1)} %bitcast.90, bf16[1,2048,512]{2,1,0:T(8,128)(2,1)S(1)} %copy-done), kind=kOutput, calls=%fused_computation.16 | convolution fusion | flops 1610612736 | bytes 6815744 | tf_op jit(solution)/shard_map/dot_general | solution.py:114
  115.9 2.9 fusion.6
  118.9 2.4 all-gather.7.cloned.1.call-done
  121.3 5.7 %multiply_convert_fusion.1 = (bf16[768,512]{1,0:T(8,128)(2,1)S(1)}, bf16[768,512]{1,0:T(8,128)(2,1)S(1)}) fusion(f32[768,512]{1,0:T(8,128)} %fusion.3, f32[768,512]{1,0:T(8,128)} %fusion.6, bf16[768,2048]{1,0:T(8,128)(2,1)} %bitcast.94, bf16[1,512,2048]{2,1,0:T(8,128)(2,1)} %param.23), kind=kOutput, calls=%fused_computation.30 | convolution fusion | flops 1615724544 | bytes 9961472 | tf_op jit(solution)/shard_map/dot_general | solution.py:39
  127.0 1.8 fusion.1
  129.1 3.5 add_convert_fusion
  132.7 24.6 %all-reduce.20.cloned.1.call-done = bf16[16,48,2048]{2,1,0:T(8,128)(2,1)} async-done(((bf16[16,48,2048]{2,1,0:T(8,128)(2,1)}), bf16[16,48,2048]{2,1,0:T(8,128)(2,1)}) %all-reduce.20.cloned.1.call-update) | async-done | bytes 3145744 | tf_op jit(solution)/shard_map/psum | solution.py:131
  157.3 6.8 %all-to-all-start.2 = ((bf16[16,48,2048]{2,1,0:T(8,128)(2,1)}), bf16[16,48,2048]{2,1,0:T(8,128)(2,1)S(1)}, u32[]{:S(2)}, u32[]{:S(2)}) async-start(bf16[16,48,2048]{2,1,0:T(8,128)(2,1)} %all-reduce.20.cloned.1.call-done), calls=%async_computation.2 | async-start | bytes 6291456 | tf_op jit(solution)/shard_map/all_to_all | solution.py:132
  164.4 61.0 %all-to-all-done.2 = bf16[16,48,2048]{2,1,0:T(8,128)(2,1)S(1)} async-done(((bf16[16,48,2048]{2,1,0:T(8,128)(2,1)}), bf16[16,48,2048]{2,1,0:T(8,128)(2,1)S(1)}, u32[]{:S(2)}, u32[]{:S(2)}) %all-to-all-start.2) | async-done | bytes 3145760 | tf_op jit(solution)/shard_map/all_to_all | solution.py:132
  225.4 3.1 gather_fusion.2
  228.5 3.4 reshape.112
  231.9 5.6 %reduce_sum.31 = f32[192,2048]{1,0:T(8,128)} reduce(f32[192,2,2048]{2,1,0:T(2,128)S(1)} %reshape.112, f32[]{:T(128)} %constant.83.clone.1), dimensions={1}, to_apply=%region_6.7 | reduce | flops 393216 | bytes 4718596 | tf_op jit(solution)/shard_map/reduce_sum | solution.py:134
  237.5 6.4 %fusion.23 = f32[2048,1024]{1,0:T(8,128)} fusion(bf16[192,1024]{1,0:T(8,128)(2,1)} %param.17, bf16[192,1024]{1,0:T(8,128)(2,1)S(1)} %copy-done.5, f32[192,2048]{1,0:T(8,128)} %reduce_sum.31, bf16[192,2048]{1,0:T(8,128)(2,1)} %param.14), kind=kOutput, calls=%fused_computation.50 | convolution fusion | flops 808845312 | bytes 11534336 | tf_op jit(solution)/shard_map/dot_general | solution.py:33
  244.0 5.1 %collective-permute-start = (bf16[1,1024]{1,0:T(2,128)(2,1)S(1)}, bf16[1,1024]{1,0:T(2,128)(2,1)S(1)}, u32[]{:S(2)}, u32[]{:S(2)}) collective-permute-start(bf16[1,1024]{1,0:T(2,128)(2,1)S(1)} %slice.282), channel_id=1, source_target_pairs={{0,2},{2,4},{4,6},{6,8},{8,10},{10,12},{12,14},{14,16},{16,18},{18... | collective-permute-start | bytes 6152 | tf_op jit(solution)/shard_map/ppermute | solution.py:29
  249.1 1.5 rev.19
  250.6 1.0 fusion.56
  251.7 0.8 fusion.12
  252.7 48.0 %all-gather = f32[16384]{0:T(1024)S(1)} all-gather(f32[1024]{0:T(1024)S(1)} %exp.25), channel_id=2, replica_groups=mesh['sp'=16,'tp'=2] {'sp'}, dimensions={0}, use_global_device_ids=true | all-gather | bytes 69632 | tf_op jit(solution)/shard_map/all_gather | solution.py:12
  300.7 1.2 slice.292
  302.0 1.4 slice.221
  303.4 1.4 slice.228
  304.8 1.4 slice.219
  306.2 1.0 slice.321
  307.2 4.6 %slice.222 = f32[96,1024]{1,0:T(8,128)} reverse(f32[96,1024]{1,0:T(8,128)} %slice.221), dimensions={0} | reverse | bytes 786432 | tf_op jit(solution)/shard_map/slice | solution.py:50
  311.8 2.6 slice.229
  314.3 2.6 slice.220
  317.0 2.4 rev.21
  319.8 5.3 %rev.20 = f32[192,1024]{1,0:T(8,128)} reverse(f32[192,1024]{1,0:T(8,128)S(1)} %slice.317), dimensions={0} | reverse | bytes 1572864 | tf_op jit(solution)/shard_map/jit(_flip)/rev | solution.py:155
  325.1 5.9 %convolution_bitcast_fusion.1 = f32[1,2048,512]{2,1,0:T(8,128)} fusion(bf16[768,2048]{1,0:T(8,128)(2,1)} %bitcast.91, bf16[768,512]{1,0:T(8,128)(2,1)S(1)} %copy-done.15), kind=kOutput, calls=%fused_computation.10 | convolution fusion | flops 1610612736 | bytes 8126464 | tf_op jit(solution)/shard_map/dot_general | solution.py:33
  331.1 3.9 convolution_bitcast_fusion.2
  335.0 4.1 convolution_bitcast_fusion
  339.1 2.7 fusion.22
  342.2 2.6 slice.224
  344.8 2.6 slice.226
  347.4 1.2 fusion.57
  349.7 1.0 fusion.58
  358.6 1.1 fusion.24
  359.9 1.0 add.218
  361.6 39.2 %all-gather.1 = f32[16,1,1024]{2,1,0:T(1,128)S(1)} all-gather(f32[1,1,1024]{2,1,0:T(1,128)S(1)} %fusion.41), channel_id=1, replica_groups=mesh['sp'=16,'tp'=2] {'sp'}, dimensions={0}, use_global_device_ids=true | all-gather | bytes 69632 | tf_op jit(solution)/shard_map/all_gather | solution.py:12
  401.0 8.6 %rev.18 = f32[192,1024]{1,0:T(8,128)} reverse(f32[192,1024]{1,0:T(8,128)} %add.218), dimensions={0} | reverse | bytes 1572864 | tf_op jit(solution)/shard_map/jit(_flip)/rev | solution.py:51
  409.5 11.9 %while.14 = (s32[]{:T(128)}, f32[1024]{0:T(1024)S(1)}, s32[]{:T(128)}, f32[16,1024]{1,0:T(8,128)}, f32[16,1024]{1,0:T(8,128)S(1)}, /*index=5*/s32[]{:T(128)}, s32[]{:T(128)}) while((s32[]{:T(128)}, f32[1024]{0:T(1024)S(1)}, s32[]{:T(128)}, f32[16,1024]{1,0:T(8,128)}, f32[16,1024]{1,0:T(8,128)S(1)}, /*index=5*/s32[]{:T(128)}, ...), condition=%wide.region_12.13_spmd.clone, body=%wide.region_11.12_spmd.clone.sunk | while | flops 4100 | bytes 32869 | solution.py:23
  410.3 0.8 constant_dynamic-slice_fusion.4
  411.1 0.8 constant_dynamic-slice_fusion.4
  411.9 0.8 constant_dynamic-slice_fusion.4
  412.7 0.8 constant_dynamic-slice_fusion.4
  413.5 0.8 constant_dynamic-slice_fusion.4
  414.3 0.8 constant_dynamic-slice_fusion.4
  417.5 0.8 constant_dynamic-slice_fusion.4
  419.9 0.8 constant_dynamic-slice_fusion.4
  421.5 3.3 maximum_multiply_fusion
  424.8 10.2 %reduce-scatter.2.cloned.1.call-done = f32[128,1024]{1,0:T(8,128)} async-done(((f32[2048,1024]{1,0:T(8,128)}), f32[128,1024]{1,0:T(8,128)}) %reduce-scatter.2.cloned.1.call-update) | async-done | bytes 524304 | tf_op jit(solution)/shard_map/reduce_scatter | solution.py:142
  (202 shorter events, 19.4 us)
Async XLA Ops:
  7.2 103.8 %copy-start = (bf16[1,2048,512]{2,1,0:T(8,128)(2,1)S(1)}, bf16[1,2048,512]{2,1,0:T(8,128)(2,1)}, u32[]{:S(2)}) copy-start(bf16[1,2048,512]{2,1,0:T(8,128)(2,1)} %param.21) | copy-start | bytes 6291460
  21.8 42.6 %all-to-all-start = ((bf16[16,48,1024]{2,1,0:T(8,128)(2,1)}), bf16[16,48,1024]{2,1,0:T(8,128)(2,1)}, u32[]{:S(2)}, u32[]{:S(2)}) async-start(bf16[16,48,1024]{2,1,0:T(8,128)(2,1)} %constant_dynamic-slice_fusion.2), calls=%async_computation | async-start | bytes 3145728 | tf_op jit(solution)/shard_map/all_to_all | solution.py:99
  30.1 80.8 %all-gather.5.cloned.1.call-start = ((), (), s32[]{:S(2)}) async-start(), calls=%async_computation.4 | async-start | bytes 4718592 | tf_op jit(solution)/shard_map/all_gather | solution.py:103
  31.4 4.2 copy-start.23
  64.3 56.9 %all-gather.7.cloned.1.call-start = ((), (), s32[]{:S(2)}) async-start(), calls=%async_computation.5 | async-start | bytes 4718592 | tf_op jit(solution)/shard_map/all_gather | solution.py:104
  110.7 46.6 %all-reduce.20.cloned.1.call-start = ((), (), s32[]{:S(2)}) async-start(), calls=%async_computation.6 | async-start | bytes 6291456 | tf_op jit(solution)/shard_map/psum | solution.py:131
  110.9 5.0 %copy-start.6 = (bf16[1,2048,512]{2,1,0:T(8,128)(2,1)S(1)}, bf16[1,2048,512]{2,1,0:T(8,128)(2,1)}, u32[]{:S(2)}) copy-start(bf16[1,2048,512]{2,1,0:T(8,128)(2,1)} %param.22) | copy-start | bytes 6291460
  110.9 5.0 %copy-start.25 = (bf16[16,48,2048]{2,1,0:T(8,128)(2,1)S(1)}, bf16[16,48,2048]{2,1,0:T(8,128)(2,1)}, u32[]{:S(2)}) copy-start(bf16[16,48,2048]{2,1,0:T(8,128)(2,1)} %all-gather.5.cloned.1.call-done) | copy-start | bytes 9437188
  127.0 1.9 copy-start.12
  127.0 1.9 copy-start.14
  127.0 2.2 copy-start.7
  157.3 68.1 %all-to-all-start.2 = ((bf16[16,48,2048]{2,1,0:T(8,128)(2,1)}), bf16[16,48,2048]{2,1,0:T(8,128)(2,1)S(1)}, u32[]{:S(2)}, u32[]{:S(2)}) async-start(bf16[16,48,2048]{2,1,0:T(8,128)(2,1)} %all-reduce.20.cloned.1.call-done), calls=%async_computation.2 | async-start | bytes 6291456 | tf_op jit(solution)/shard_map/all_to_all | solution.py:132
  164.1 270.9 %reduce-scatter.2.cloned.1.call-start = ((), (), s32[]{:S(2)}) async-start(), calls=%async_computation.7 | async-start | bytes 8912896 | tf_op jit(solution)/shard_map/reduce_scatter | solution.py:142
  231.9 5.6 %copy-start.5 = (bf16[192,1024]{1,0:T(8,128)(2,1)S(1)}, bf16[192,1024]{1,0:T(8,128)(2,1)}, u32[]{:S(2)}) copy-start(bf16[192,1024]{1,0:T(8,128)(2,1)} %param.18) | copy-start | bytes 1179652
  243.9 5.2 %copy-start.3 = (f32[192,1024]{1,0:T(8,128)S(1)}, f32[192,1024]{1,0:T(8,128)}, u32[]{:S(2)}) copy-start(f32[192,1024]{1,0:T(8,128)} %param.19) | copy-start | bytes 2359300
  244.0 81.1 %collective-permute-start = (bf16[1,1024]{1,0:T(2,128)(2,1)S(1)}, bf16[1,1024]{1,0:T(2,128)(2,1)S(1)}, u32[]{:S(2)}, u32[]{:S(2)}) collective-permute-start(bf16[1,1024]{1,0:T(2,128)(2,1)S(1)} %slice.282), channel_id=1, source_target_pairs={{0,2},{2,4},{4,6},{6,8},{8,10},{10,12},{12,14},{14,16},{16,18},{18... | collective-permute-start | bytes 6152 | tf_op jit(solution)/shard_map/ppermute | solution.py:29
  306.2 5.5 %copy-start.11 = (f32[96,1024]{1,0:T(8,128)S(1)}, f32[96,1024]{1,0:T(8,128)}, u32[]{:S(2)}) copy-start(f32[96,1024]{1,0:T(8,128)} %slice.228) | copy-start | bytes 1179652
  306.2 8.1 %copy-start.10 = (f32[95,1024]{1,0:T(8,128)S(1)}, f32[95,1024]{1,0:T(8,128)}, u32[]{:S(2)}) copy-start(f32[95,1024]{1,0:T(8,128)} %slice.219) | copy-start | bytes 1167364
  319.8 5.4 %copy-start.15 = (bf16[768,512]{1,0:T(8,128)(2,1)S(1)}, bf16[768,512]{1,0:T(8,128)(2,1)}, u32[]{:S(2)}) copy-start(bf16[768,512]{1,0:T(8,128)(2,1)} %copy-done.14) | copy-start | bytes 2359300
  325.1 5.9 %copy-start.13 = (bf16[768,512]{1,0:T(8,128)(2,1)S(1)}, bf16[768,512]{1,0:T(8,128)(2,1)}, u32[]{:S(2)}) copy-start(bf16[768,512]{1,0:T(8,128)(2,1)} %copy-done.12) | copy-start | bytes 2359300
  325.1 5.9 %copy-start.26 = (bf16[16,48,2048]{2,1,0:T(8,128)(2,1)S(1)}, bf16[16,48,2048]{2,1,0:T(8,128)(2,1)}, u32[]{:S(2)}) copy-start(bf16[16,48,2048]{2,1,0:T(8,128)(2,1)} %all-gather.5.cloned.1.call-done) | copy-start | bytes 9437188
  331.1 3.9 copy-start.27
  331.1 3.9 copy-start.28
  331.1 3.9 copy-start.29
  335.0 4.1 copy-start.2
  335.0 4.1 copy-start.4
  335.0 4.1 copy-start.16
  335.0 4.1 copy-start.24
  341.8 5.5 %copy-start.8 = (f32[96,1024]{1,0:T(8,128)S(1)}, f32[96,1024]{1,0:T(8,128)}, u32[]{:S(2)}) copy-start(f32[96,1024]{1,0:T(8,128)} %slice.222) | copy-start | bytes 1179652
  341.8 5.5 %copy-start.9 = (f32[96,1024]{1,0:T(8,128)S(1)}, f32[96,1024]{1,0:T(8,128)}, u32[]{:S(2)}) copy-start(f32[96,1024]{1,0:T(8,128)} %slice.229) | copy-start | bytes 1179652
  352.5 3.9 copy-start.17
  353.8 2.6 copy-start.22
  354.7 2.7 copy-start.21
  354.7 2.8 copy-start.20
  357.3 0.7 copy-start.19
  358.1 1.6 copy-start.18
  421.5 13.6 %copy-start.1 = (bf16[1,2048,512]{2,1,0:T(8,128)(2,1)S(1)}, bf16[1,2048,512]{2,1,0:T(8,128)(2,1)}, u32[]{:S(2)}) copy-start(bf16[1,2048,512]{2,1,0:T(8,128)(2,1)} %param.21) | copy-start | bytes 6291460
Sparse Core Ops, SparseCore 0:
  64.5 14.2 all-gather.4
  110.8 10.4 all-gather.6
  132.8 24.4 all-reduce.19
  244.1 190.8 reduce-scatter.1
where the time goes:
time: 446 us; the launch traced here: 442 us
  blocking collectives  132 us (30%)
  waiting for transfers between devices  124 us (28%)
  local copies, waits for them, and re-layouts  87.8 us (20%)
  matrix products  41.9 us (9%)
  starting transfers between devices  20.9 us (5%)
  other arithmetic  20.7 us (5%)
  between operations  14.7 us (3%)
    all_gather x2, blocking collectives, entering(): pieces = jax.tree.map(lambda part: lax.all_gather(part, axis), value)  87.2 us
    all_to_all x1, waiting for transfers between devices, on_device(): lax.all_to_all(summed_back, 'sp', split_axis=0, concat_axis=0, tiled=True)  61 us
    all_to_all x1, blocking collectives, on_device(): lax.all_to_all(cot_piece, 'sp', split_axis=0, concat_axis=0, tiled=True)  44.5 us
    slice x48, local copies, waits for them, and re-layouts, local_recurrence(): lax.associative_scan(combine, (jnp.flip(coeffs, 0), jnp.flip(drive, 0)),...  26.3 us
    all_to_all x1, waiting for transfers between devices, on_device(): lax.all_to_all(rows_piece, 'sp', split_axis=0, concat_axis=0, tiled=True)  25.4 us
    psum x1, waiting for transfers between devices, on_device(): lax.psum(back_stack, 'tp').astype(jnp.float32).astype(jnp.bfloat16)  24.6 us
    dot_general x4, matrix products, contract_rows(): lax.dot_general(left, right, (((0,), (0,)), ((), ())), preferred_element_...  20.3 us
    dot_general x4, matrix products, contract_cols(): lax.dot_general(left, right, (((1,), (1,)), ((), ())), preferred_element_...  13.7 us
  transfers between devices with their start and end apart: 7, of which 5 were waited for; matrix products, arithmetic and copies ran while one was open for 24% of the time, Pallas kernels for 0%

commit v1 on v0

v1 whole, which is shorter than its diff:
```python
import functools

import jax
import jax.numpy as jnp
from jax import lax
from jax.experimental import pallas as pl
from jax.experimental.pallas import tpu as pltpu
from jax.sharding import PartitionSpec as P

TOPK = 2
EXP_DEV = 1
GELU_SCALE = 0.7978845608028654
GELU_CUBIC = 0.044715


def shifted(value, axis, steps):
    count = lax.axis_size(axis)
    leading, last = (max(0, -steps), min(count, count - steps))
    return lax.ppermute(value, axis, [(source, source + steps) for source in range(leading, last)])


def swapped(value):
    return lax.ppermute(value, "tp", [(0, 1), (1, 0)])


def contract_rows(left, right):
    return lax.dot_general(
        left, right, (((0,), (0,)), ((), ())), preferred_element_type=jnp.float32
    )


def contract_cols(left, right):
    return lax.dot_general(
        left, right, (((1,), (1,)), ((), ())), preferred_element_type=jnp.float32
    )


def dot(left, right):
    return jnp.dot(left, right, preferred_element_type=jnp.float32)


def gelu_parts(value):
    squared = value * value
    bent = jnp.tanh(GELU_SCALE * (value + GELU_CUBIC * squared * value))
    half = 0.5 * (1.0 + bent)
    slope = half + 0.5 * value * (1.0 - bent * bent) * GELU_SCALE * (
        1.0 + 3.0 * GELU_CUBIC * squared
    )
    return value * half, slope


def local_kernel(mid_ref, w_ref, pre_ref, state_ref, log_ref, gate_ref, grad_ref, coef_ref, edge_ref):
    d_gated = contract_cols(mid_ref[...], w_ref[...])
    value, slope = gelu_parts(pre_ref[...].astype(jnp.float32))
    gate_ref[...] = (d_gated * state_ref[...].astype(jnp.float32) * slope).astype(jnp.bfloat16)
    decay = jnp.exp(log_ref[...])
    rows, width = decay.shape
    grad = d_gated * value
    coef = jnp.concatenate([decay[1:], jnp.ones((1, width), jnp.float32)], axis=0)
    step = 1
    while step < rows:
        later_grad = jnp.concatenate(
            [grad[step:], jnp.zeros((step, width), jnp.float32)], axis=0
        )
        later_coef = jnp.concatenate([coef[step:], jnp.ones((step, width), jnp.float32)], axis=0)
        grad = grad + coef * later_grad
        coef = coef * later_coef
        step *= 2
    grad_ref[...] = grad
    coef_ref[...] = coef
    edge_ref[0:1, :] = decay[0:1] * coef[0:1]
    edge_ref[1:2, :] = decay[0:1] * grad[0:1]


def local_part(d_mid, w_out, gate_pre, lru_out, log_decay):
    rows, model_width = d_mid.shape
    width = lru_out.shape[1]
    block = 256 if width % 256 == 0 else width
    narrow = pl.BlockSpec((rows, block), lambda i: (0, i))
    return pl.pallas_call(
        local_kernel,
        grid=(width // block,),
        in_specs=[
            pl.BlockSpec((rows, model_width), lambda i: (0, 0)),
            pl.BlockSpec((block, model_width), lambda i: (i, 0)),
            narrow,
            narrow,
            narrow,
        ],
        out_specs=[narrow, narrow, narrow, pl.BlockSpec((2, block), lambda i: (0, i))],
        out_shape=[
            jax.ShapeDtypeStruct((rows, width), jnp.bfloat16),
            jax.ShapeDtypeStruct((rows, width), jnp.float32),
            jax.ShapeDtypeStruct((rows, width), jnp.float32),
            jax.ShapeDtypeStruct((2, width), jnp.float32),
        ],
        cost_estimate=pl.CostEstimate(
            flops=2 * rows * width * model_width, bytes_accessed=8 << 20, transcendentals=0
        ),
    )(d_mid, w_out, gate_pre, lru_out, log_decay)


def finish_kernel(count, mine_ref, edges_ref, grad_ref, coef_ref, log_ref, prev_ref, before_ref, drive_ref, out_ref):
    mine = mine_ref[0]
    width = grad_ref.shape[1]
    carry = jnp.zeros((1, width), jnp.float32)
    for position in range(count - 1, 0, -1):
        longer = edges_ref[position, 1:2, :] + edges_ref[position, 0:1, :] * carry
        carry = jnp.where(position > mine, longer, carry)
    drive = grad_ref[...] + coef_ref[...] * carry
    drive_ref[...] = drive
    states = prev_ref[...].astype(jnp.float32)
    prev = jnp.concatenate([before_ref[...].astype(jnp.float32), states[:-1]], axis=0)
    out_ref[...] = drive * jnp.exp(log_ref[...]) * prev


def finish_part(mine, edges, grad, coef, log_decay, lru_out, before_row):
    rows, width = grad.shape
    count = edges.shape[0]
    block = 256 if width % 256 == 0 else width
    narrow = pl.BlockSpec((rows, block), lambda i: (0, i))
    return pl.pallas_call(
        functools.partial(finish_kernel, count),
        grid=(width // block,),
        in_specs=[
            pl.BlockSpec(memory_space=pltpu.SMEM),
            pl.BlockSpec((count, 2, block), lambda i: (0, 0, i)),
            narrow,
            narrow,
            narrow,
            narrow,
            pl.BlockSpec((1, block), lambda i: (0, i)),
        ],
        out_specs=[narrow, narrow],
        out_shape=[jax.ShapeDtypeStruct((rows, width), jnp.float32)] * 2,
        cost_estimate=pl.CostEstimate(
            flops=8 * rows * width, bytes_accessed=5 << 20, transcendentals=0
        ),
    )(mine, edges, grad, coef, log_decay, lru_out, before_row)


def on_device(
    stream_mid,
    d_out,
    route_ids,
    route_weights,
    gate_pre,
    lru_out,
    log_decay,
    w_out,
    exp_gate,
    exp_up,
    exp_down,
):
    rows_local = d_out.shape[0]
    model_width = d_out.shape[1]
    sp_count = lax.axis_size("sp")
    tp_index = lax.axis_index("tp")
    lines = 4 if sp_count % 4 == 0 else 1
    plane = sp_count // lines
    plane_groups = [[line * plane + place for place in range(plane)] for line in range(lines)]
    line_groups = [[line * plane + place for line in range(lines)] for place in range(plane)]
    expert_count = EXP_DEV * sp_count
    capacity = max(2, 2 * rows_local * TOPK // expert_count)
    slot_count = expert_count * capacity
    half_cols = model_width // 2
    own_start = tp_index * half_cols
    other_start = half_cols - own_start

    experts = jnp.arange(expert_count, dtype=jnp.int32)[None, :]
    slots = jnp.arange(slot_count, dtype=jnp.int32)[None, :]
    places = jnp.arange(rows_local, dtype=jnp.int32)
    earlier = (places[None, :] < places[:, None]).astype(jnp.bfloat16)
    hits = []
    before = jnp.zeros((1, expert_count), jnp.float32)
    for pick in range(TOPK):
        chosen = route_ids[:, pick : pick + 1]
        onehot = (chosen == experts).astype(jnp.bfloat16)
        wide = onehot.astype(jnp.float32)
        rank = dot(earlier, onehot) + before
        before = before + jnp.sum(wide, axis=0, keepdims=True)
        place = jnp.sum(rank * wide, axis=1, keepdims=True).astype(jnp.int32)
        hits.append(slots == chosen * capacity + place)
    any_hit = (hits[0] | hits[1]).astype(jnp.bfloat16)
    each_hit = jnp.concatenate([hit.astype(jnp.bfloat16) for hit in hits], axis=0)
    stream_half = lax.dynamic_slice_in_dim(stream_mid, own_start, half_cols, 1)
    cot_half = lax.dynamic_slice_in_dim(d_out, own_start, half_cols, 1)
    cot_wide = cot_half.astype(jnp.float32)
    scaled = jnp.concatenate(
        [
            (route_weights[:, pick : pick + 1] * cot_wide).astype(jnp.bfloat16)
            for pick in range(TOPK)
        ],
        axis=0,
    )
    rows_piece = contract_rows(any_hit, stream_half).astype(jnp.bfloat16)
    cot_piece = contract_rows(each_hit, scaled).astype(jnp.bfloat16)
    rows_piece = rows_piece.reshape(sp_count, EXP_DEV * capacity, half_cols)
    cot_piece = cot_piece.reshape(sp_count, EXP_DEV * capacity, half_cols)
    got_rows = lax.all_to_all(rows_piece, "sp", split_axis=0, concat_axis=0, tiled=True)
    got_cot = lax.all_to_all(cot_piece, "sp", split_axis=0, concat_axis=0, tiled=True)
    inputs = lax.all_gather(got_rows, "tp", axis=2, tiled=True).reshape(slot_count, model_width)
    cotangent = lax.all_gather(got_cot, "tp", axis=2, tiled=True).reshape(slot_count, model_width)

    gate_value, _ = gelu_parts(gate_pre.astype(jnp.float32))
    gated = (gate_value * lru_out.astype(jnp.float32)).astype(jnp.bfloat16)
    plane_gated = lax.all_gather(gated, "sp", axis=0, tiled=True, axis_index_groups=plane_groups)
    before_row = shifted(lru_out[-1:], "sp", 1)

    gate_proj = dot(inputs, exp_gate[0])
    up_proj = dot(inputs, exp_up[0])
    gate_sigmoid = jax.nn.sigmoid(gate_proj)
    gate_act = gate_proj * gate_sigmoid
    hidden = (gate_act * up_proj).astype(jnp.bfloat16)
    back_hidden = contract_cols(cotangent, exp_down[0])
    grad_gate_pre = (
        back_hidden * up_proj * gate_sigmoid * (1.0 + gate_proj * (1.0 - gate_sigmoid))
    ).astype(jnp.bfloat16)
    grad_up_pre = (back_hidden * gate_act).astype(jnp.bfloat16)

    def back_piece(start):
        gate_rows = lax.dynamic_slice_in_dim(exp_gate[0], start, half_cols, 0)
        up_rows = lax.dynamic_slice_in_dim(exp_up[0], start, half_cols, 0)
        piece = contract_cols(grad_gate_pre, gate_rows) + contract_cols(grad_up_pre, up_rows)
        return piece.astype(jnp.bfloat16)

    from_other = swapped(back_piece(other_start))
    own_piece = back_piece(own_start)
    summed_back = (own_piece.astype(jnp.float32) + from_other.astype(jnp.float32)).astype(
        jnp.bfloat16
    )
    summed_back = summed_back.reshape(sp_count, EXP_DEV * capacity, half_cols)
    returned = lax.all_to_all(summed_back, "sp", split_axis=0, concat_axis=0, tiled=True)
    routed_back = dot(any_hit, returned.reshape(slot_count, half_cols))
    mid_half = (cot_wide + routed_back).astype(jnp.bfloat16)
    mid_other = swapped(mid_half)
    first = tp_index == 0
    d_mid = jnp.concatenate(
        [jnp.where(first, mid_half, mid_other), jnp.where(first, mid_other, mid_half)], axis=1
    )

    down_grad = contract_rows(hidden, cotangent)
    gate_grad = contract_rows(inputs, grad_gate_pre)
    up_grad = contract_rows(inputs, grad_up_pre)

    share = model_width // sp_count
    mid_pieces = jnp.stack(
        [
            jnp.concatenate(
                [
                    d_mid[:, (line * plane + place) * share : (line * plane + place + 1) * share]
                    for line in range(lines)
                ],
                axis=1,
            )
            for place in range(plane)
        ],
        axis=0,
    )
    mid_pieces = lax.all_to_all(
        mid_pieces, "sp", split_axis=0, concat_axis=0, tiled=True, axis_index_groups=plane_groups
    )
    mid_rows = mid_pieces.reshape(plane * rows_local, lines * share)
    partial = contract_rows(mid_rows, plane_gated).astype(jnp.bfloat16)
    grad_out_proj = lax.psum_scatter(
        partial, "sp", scatter_dimension=0, tiled=True, axis_index_groups=line_groups
    ).astype(jnp.float32)

    d_gate, local_grad, coef, edge = local_part(d_mid, w_out, gate_pre, lru_out, log_decay)
    edges = lax.all_gather(edge, "sp")
    mine = lax.axis_index("sp").reshape(1).astype(jnp.int32)
    d_drive, d_log_decay = finish_part(
        mine, edges, local_grad, coef, log_decay, lru_out, before_row
    )
    return (
        gate_grad[None],
        up_grad[None],
        down_grad[None],
        grad_out_proj,
        d_gate,
        d_drive,
        d_log_decay,
    )


def solution(mesh):
    in_specs = (
        P("sp", None),
        P("sp", None),
        P("sp", None),
        P("sp", None),
        P("sp", "tp"),
        P("sp", "tp"),
        P("sp", "tp"),
        P("tp", None),
        P("sp", None, "tp"),
        P("sp", None, "tp"),
        P("sp", "tp", None),
    )
    out_specs = (
        P("sp", None, "tp"),
        P("sp", None, "tp"),
        P("sp", "tp", None),
        P("sp", "tp"),
        P("sp", "tp"),
        P("sp", "tp"),
        P("sp", "tp"),
    )
    return jax.shard_map(
        on_device, mesh=mesh, in_specs=in_specs, out_specs=out_specs, check_vma=False
    )
```

time: 446 us -> 274 us (0.61)
  local copies, waits for them, and re-layouts: 87.8 us -> 3.39 us
  blocking collectives: 132 us -> 86.1 us
  waiting for transfers between devices: 124 us -> 83.6 us
  other arithmetic: 20.7 us -> 7.27 us
  Pallas kernels: 0 us -> 11 us
    all_gather x2 -> x1, blocking collectives: 87.2 us -> 41.6 us  [on_device(): edges = lax.all_gather(edge, 'sp')]
    all_to_all x1, waiting for transfers between devices: 61 us -> 32.9 us  [on_device(): lax.all_to_all(summed_back, 'sp', split_axis=0, concat_axis=0, tiled=True)]
    slice x51 -> x4, local copies, waits for them, and re-layouts: 28.7 us -> 1 us  [the longest x1 0.85 us: on_device(): chosen = route_ids[:, pick:pick + 1]]
    psum x1 -> x0, waiting for transfers between devices: 24.6 us -> none  [on_device(): lax.psum(back_stack, 'tp').astype(jnp.float32).astype(jnp.bfloat16)]
    rev x5 -> x0, local copies, waits for them, and re-layouts: 17.9 us -> none  [the longest x1 8.58 us: local_recurrence(): return jnp.flip(carried, 0)]
    dynamic_slice x16 -> x0, local copies, waits for them, and re-layouts: 14.3 us -> none  [the longest x15 11.6 us: turn(): longer = join(subtotal, jax.tree.map(lambda part: part[position], pieces))]
    gather x3 -> x0, local copies, waits for them, and re-layouts: 11.6 us -> none  [the longest x1 4.23 us: on_device(): padded_stream[source].reshape(sp_count, EXP_DEV * capacity, model_width)]
    pallas_call x0 -> x2, Pallas kernels: none -> 11 us  [the longest x1 7.01 us: local_part(): pl.pallas_call(local_kernel, grid=(width // block,), in_specs=[pl.BlockSp...]
  transfers between devices with their start and end apart: 7 -> 10, of which waited for: 5 -> 7; matrix products, arithmetic and copies ran while one was open for 24% -> 11% of each run, Pallas kernels for 0% -> 4%
where the time goes in v1:
time: 274 us; the launch traced here: 273 us
  blocking collectives  86.1 us (31%)
  waiting for transfers between devices  83.6 us (31%)
  matrix products  42.2 us (15%)
  starting transfers between devices  23.8 us (9%)
  between operations  15.8 us (6%)
  Pallas kernels  11 us (4%)
  other arithmetic  7.27 us (3%)
  local copies, waits for them, and re-layouts  3.39 us (1%)
    all_to_all x1, blocking collectives, on_device(): lax.all_to_all(cot_piece, 'sp', split_axis=0, concat_axis=0, tiled=True)  44.5 us
    all_gather x1, blocking collectives, on_device(): edges = lax.all_gather(edge, 'sp')  41.6 us
    all_to_all x1, waiting for transfers between devices, on_device(): lax.all_to_all(summed_back, 'sp', split_axis=0, concat_axis=0, tiled=True)  32.9 us
    all_to_all x1, waiting for transfers between devices, on_device(): lax.all_to_all(rows_piece, 'sp', split_axis=0, concat_axis=0, tiled=True)  32.9 us
    dot_general x6, matrix products, contract_rows(): lax.dot_general(left, right, (((0,), (0,)), ((), ())), preferred_element_...  21.4 us
    dot_general x5, matrix products, contract_cols(): lax.dot_general(left, right, (((1,), (1,)), ((), ())), preferred_element_...  10.9 us
    dot_general x5, matrix products, dot(): return jnp.dot(left, right, preferred_element_type=jnp.float32)  9.86 us
    all_to_all x1, waiting for transfers between devices, on_device(): lax.all_to_all(mid_pieces, 'sp', split_axis=0, concat_axis=0, tiled=True,...  9 us
  transfers between devices with their start and end apart: 10, of which 7 were waited for; matrix products, arithmetic and copies ran while one was open for 11% of the time, Pallas kernels for 4%

profile of v1, /device:TPU:0, one launch (start us, length us, event | category | flops | bytes accessed | tf_op | source)
XLA Modules:
  0.0 273.1 jit_solution(13615176224426424806)
XLA Ops:
  8.0 0.0 copy-start
  8.0 0.9 fusion.56
  8.9 0.1 convert_reduce_fusion
  9.0 0.2 fusion.12
  9.2 0.2 fusion.13
  9.4 0.8 multiply_add_fusion
  10.1 2.9 %convolution_convert_fusion = bf16[768,1024]{1,0:T(8,128)(2,1)} fusion(bf16[192,2048]{1,0:T(8,128)(2,1)} %param.11, s32[]{:T(128)S(6)} %select_n.22, s32[192]{0:T(256)S(1)} %bitcast.76, s32[192]{0:T(256)S(1)} %bitcast.73), kind=kOutput, calls=%fused_computation.12 | convolution fusion | flops 303218688 | bytes 1967620 | tf_op jit(solution)/shard_map/dot_general | solution.py:27
  13.0 8.4 %all-to-all-start = ((bf16[16,48,1024]{2,1,0:T(8,128)(2,1)}), bf16[16,48,1024]{2,1,0:T(8,128)(2,1)}, u32[]{:S(2)}, u32[]{:S(2)}) async-start(bf16[16,48,1024]{2,1,0:T(8,128)(2,1)} %bitcast.69), calls=%async_computation | async-start | bytes 3145728 | tf_op jit(solution)/shard_map/all_to_all | solution.py:200
  21.4 0.0 all-gather.6.cloned.1.call-start
  21.5 0.0 copy-done.10
  21.5 1.2 fusion.24
  22.7 32.9 %all-to-all-done = bf16[16,48,1024]{2,1,0:T(8,128)(2,1)} async-done(((bf16[16,48,1024]{2,1,0:T(8,128)(2,1)}), bf16[16,48,1024]{2,1,0:T(8,128)(2,1)}, u32[]{:S(2)}, u32[]{:S(2)}) %all-to-all-start) | async-done | bytes 1572896 | tf_op jit(solution)/shard_map/all_to_all | solution.py:200
  55.6 0.0 all-gather.6.cloned.1.call-update
  55.6 0.0 all-gather.8.cloned.1.call-start
  55.7 0.2 iota_compare_fusion
  55.9 1.0 convolution_convert_fusion.1
  56.9 44.5 %all_to_all.20 = bf16[16,48,1024]{2,1,0:T(8,128)(2,1)} all-to-all(bf16[16,48,1024]{2,1,0:T(8,128)(2,1)S(1)} %bitcast.71), channel_id=1, replica_groups=mesh['sp'=16,'tp'=2] {'sp'}, dimensions={0} | all-to-all | bytes 3145728 | tf_op jit(solution)/shard_map/all_to_all | solution.py:201
  101.5 0.0 all-gather.8.cloned.1.call-update
  101.5 0.0 all-gather.6.cloned.1.call-done
  101.5 0.0 copy-done
  101.5 0.0 copy-start.5
  101.5 5.0 %fusion = f32[768,512]{1,0:T(8,128)} fusion(bf16[768,2048]{1,0:T(8,128)(2,1)} %bitcast.87, bf16[1,2048,512]{2,1,0:T(8,128)(2,1)S(1)} %copy-done), kind=kOutput, calls=%fused_computation.6 | convolution fusion | flops 1610612736 | bytes 6815744 | tf_op jit(solution)/shard_map/dot_general | solution.py:39
  106.5 0.0 copy-done.5
  106.5 2.9 %fusion.2 = f32[768,512]{1,0:T(8,128)} fusion(bf16[768,2048]{1,0:T(8,128)(2,1)S(1)} %bitcast.89, bf16[1,2048,512]{2,1,0:T(8,128)(2,1)S(1)} %copy-done.5), kind=kOutput, calls=%fused_computation.8 | convolution fusion | flops 1610612736 | bytes 6815744 | tf_op jit(solution)/shard_map/dot_general | solution.py:39
  109.4 2.6 all-gather.8.cloned.1.call-done
  112.1 5.7 %multiply_convert_fusion.1 = (bf16[768,512]{1,0:T(8,128)(2,1)S(1)}, bf16[768,512]{1,0:T(8,128)(2,1)S(1)}) fusion(f32[768,512]{1,0:T(8,128)} %fusion, f32[768,512]{1,0:T(8,128)} %fusion.2, bf16[768,2048]{1,0:T(8,128)(2,1)} %bitcast.91, bf16[1,512,2048]{2,1,0:T(8,128)(2,1)} %param.21), kind=kOutput, calls=%fused_computation.15 | convolution fusion | flops 1615724544 | bytes 9961472 | tf_op jit(solution)/shard_map/dot_general | solution.py:33
  117.8 0.0 copy-start.3
  117.8 0.0 copy-start.6
  117.8 1.0 fusion.15
  118.8 0.8 copy-done.6
  119.7 1.0 add_convert_fusion.1
  120.7 0.3 collective-permute-start
  121.0 1.0 fusion.18
  122.0 2.2 collective-permute-done
  124.2 2.2 add_convert_fusion
  126.3 6.9 %all-to-all-start.2 = ((bf16[16,48,1024]{2,1,0:T(8,128)(2,1)}), bf16[16,48,1024]{2,1,0:T(8,128)(2,1)S(1)}, u32[]{:S(2)}, u32[]{:S(2)}) async-start(bf16[16,48,1024]{2,1,0:T(8,128)(2,1)} %bitcast.22), calls=%async_computation.2 | async-start | bytes 3145728 | tf_op jit(solution)/shard_map/all_to_all | solution.py:233
  133.3 0.2 all-gather.10.cloned.1.call-start
  133.5 1.1 fusion.32
  134.6 0.0 all-gather.10.cloned.1.call-update
  134.6 32.9 %all-to-all-done.2 = bf16[16,48,1024]{2,1,0:T(8,128)(2,1)S(1)} async-done(((bf16[16,48,1024]{2,1,0:T(8,128)(2,1)}), bf16[16,48,1024]{2,1,0:T(8,128)(2,1)S(1)}, u32[]{:S(2)}, u32[]{:S(2)}) %all-to-all-start.2) | async-done | bytes 1572896 | tf_op jit(solution)/shard_map/all_to_all | solution.py:233
  167.6 1.6 fusion.7
  169.2 0.1 collective-permute-start.1
  169.3 1.7 collective-permute-done.1
  171.0 0.1 broadcast_select_fusion.1
  171.0 0.1 fusion.53
  171.1 0.1 fusion.54
  171.3 1.0 pad_maximum_fusion
  172.3 4.4 %all-to-all-start.3 = ((bf16[4,192,512]{2,1,0:T(8,128)(2,1)}), bf16[4,192,512]{2,1,0:T(8,128)(2,1)S(1)}, u32[]{:S(2)}, u32[]{:S(2)}) async-start(bf16[4,192,512]{2,1,0:T(8,128)(2,1)} %pad_maximum_fusion), calls=%async_computation.3 | async-start | bytes 1572864 | tf_op jit(solution)/shard_map/all_to_all | solution.py:260
  176.7 2.2 all-gather.10.cloned.1.call-done
  179.0 9.0 %all-to-all-done.3 = bf16[4,192,512]{2,1,0:T(8,128)(2,1)S(1)} async-done(((bf16[4,192,512]{2,1,0:T(8,128)(2,1)}), bf16[4,192,512]{2,1,0:T(8,128)(2,1)S(1)}, u32[]{:S(2)}, u32[]{:S(2)}) %all-to-all-start.3) | async-done | bytes 786464 | tf_op jit(solution)/shard_map/all_to_all | solution.py:260
  188.0 0.9 copy-done.8
  188.9 3.7 %convolution_convert_fusion.2 = bf16[512,1024]{1,0:T(8,128)(2,1)} fusion(bf16[768,512]{1,0:T(8,128)(2,1)} %bitcast.72, bf16[768,1024]{1,0:T(8,128)(2,1)} %all-gather.10.cloned.1.call-done), kind=kOutput, calls=%fused_computation.19 | convolution fusion | flops 805830656 | bytes 3407872 | tf_op jit(solution)/shard_map/dot_general | solution.py:27
  192.6 0.0 reduce-scatter.2.cloned.1.call-update
  192.6 3.4 %collective-permute-start.2 = (bf16[1,1024]{1,0:T(2,128)(2,1)S(1)}, bf16[1,1024]{1,0:T(2,128)(2,1)S(1)}, u32[]{:S(2)}, u32[]{:S(2)}) collective-permute-start(bf16[1,1024]{1,0:T(2,128)(2,1)S(1)} %slice.83), channel_id=1, source_target_pairs={{0,2},{2,4},{4,6},{6,8},{8,10},{10,12},{12,14},{14,16},{16,18},{18... | collective-permute-start | bytes 6152 | tf_op jit(solution)/shard_map/ppermute | solution.py:19
  196.0 5.9 %convolution_bitcast_fusion.1 = f32[1,2048,512]{2,1,0:T(8,128)} fusion(bf16[768,2048]{1,0:T(8,128)(2,1)} %bitcast.88, bf16[768,512]{1,0:T(8,128)(2,1)S(1)} %copy-done.4), kind=kOutput, calls=%fused_computation.1 | convolution fusion | flops 1610612736 | bytes 8126464 | tf_op jit(solution)/shard_map/dot_general | solution.py:27
  201.9 3.9 %convolution_bitcast_fusion.2 = f32[1,2048,512]{2,1,0:T(8,128)} fusion(bf16[768,2048]{1,0:T(8,128)(2,1)S(1)} %bitcast.90, bf16[768,512]{1,0:T(8,128)(2,1)S(1)} %get-tuple-element.20), kind=kOutput, calls=%fused_computation.2 | convolution fusion | flops 1610612736 | bytes 8126464 | tf_op jit(solution)/shard_map/dot_general | solution.py:27
  205.8 4.0 %convolution_bitcast_fusion = f32[1,512,2048]{2,1,0:T(8,128)} fusion(bf16[768,2048]{1,0:T(8,128)(2,1)S(1)} %bitcast.92, f32[768,512]{1,0:T(8,128)S(1)} %copy-done.15, f32[768,512]{1,0:T(8,128)S(1)} %copy-done.14), kind=kOutput, calls=%fused_computation | convolution fusion | flops 1612972032 | bytes 10485760 | tf_op jit(solution)/shard_map/dot_general | solution.py:27
  209.8 0.9 pad_maximum_fusion.1.mid_ref
  210.7 7.0 %shard_map.162 = (bf16[192,1024]{1,0:T(8,128)(2,1)}, f32[192,1024]{1,0:T(8,128)}, f32[192,1024]{1,0:T(8,128)}, f32[2,1024]{1,0:T(2,128)}) custom-call(bf16[192,2048]{1,0:T(8,128)(2,1)} %pad_maximum_fusion.1.mid_ref, bf16[1024,2048]{1,0:T(8,128)(2,1)} %w_ref.1, bf16[192,1024]{1,0:T(8,128)(2,1)} %pre_ref.1, bf16[192,1024]{1,0:T(8,128)(2,1)} %prev_ref.1, ...), custom_call_target="tpu_custom_call" | custom-call | flops 805306368 | bytes 8388608 | tf_op jit(solution)/shard_map/pallas_call | solution.py:80
  217.8 41.6 %all-gather.1.edges_ref = f32[16,2,1024]{2,1,0:T(2,128)} all-gather(f32[1,2,1024]{2,1,0:T(2,128)} %bitcast.79), channel_id=2, replica_groups=mesh['sp'=16,'tp'=2] {'sp'}, dimensions={0}, use_global_device_ids=true | all-gather | bytes 139264 | tf_op jit(solution)/shard_map/all_gather | solution.py:270
  259.3 0.0 collective-permute-done.2.before_ref
  259.3 0.6 copy-done.9
  259.9 4.0 %shard_map.163 = (f32[192,1024]{1,0:T(8,128)}, f32[192,1024]{1,0:T(8,128)}) custom-call(s32[1]{0:T(128)} %bitcast.29.mine_ref, f32[16,2,1024]{2,1,0:T(2,128)} %all-gather.1.edges_ref, f32[192,1024]{1,0:T(8,128)} %get-tuple-element.15.grad_ref, f32[192,1024]{1,0:T(8,128)} %get-tuple-element.16.coef_ref, f32[192,1024]{1,0:T(8,128)} %log_ref.3, ...), custom_call_target="tpu_custom_call" | custom-call | flops 1572864 | bytes 5242880 | tf_op jit(solution)/shard_map/pallas_call | solution.py:122
  263.9 1.8 convert_element_type.127
  (32 shorter events, 0.2 us)
Async XLA Ops:
  8.0 93.5 %copy-start = (bf16[1,2048,512]{2,1,0:T(8,128)(2,1)S(1)}, bf16[1,2048,512]{2,1,0:T(8,128)(2,1)}, u32[]{:S(2)}) copy-start(bf16[1,2048,512]{2,1,0:T(8,128)(2,1)} %param.19) | copy-start | bytes 6291460
  10.1 11.3 %copy-start.10 = (f32[192,2]{0,1:T(2,128)S(1)}, f32[192,2]{0,1:T(2,128)}, u32[]{:S(2)}) copy-start(f32[192,2]{0,1:T(2,128)} %param.14) | copy-start | bytes 4612
  13.0 42.6 %all-to-all-start = ((bf16[16,48,1024]{2,1,0:T(8,128)(2,1)}), bf16[16,48,1024]{2,1,0:T(8,128)(2,1)}, u32[]{:S(2)}, u32[]{:S(2)}) async-start(bf16[16,48,1024]{2,1,0:T(8,128)(2,1)} %bitcast.69), calls=%async_computation | async-start | bytes 3145728 | tf_op jit(solution)/shard_map/all_to_all | solution.py:200
  21.4 80.1 %all-gather.6.cloned.1.call-start = ((), (), s32[]{:S(2)}) async-start(), calls=%async_computation.5 | async-start | bytes 4718592 | tf_op jit(solution)/shard_map/all_gather | solution.py:202
  55.6 56.5 %all-gather.8.cloned.1.call-start = ((), (), s32[]{:S(2)}) async-start(), calls=%async_computation.6 | async-start | bytes 4718592 | tf_op jit(solution)/shard_map/all_gather | solution.py:203
  101.5 5.0 %copy-start.5 = (bf16[1,2048,512]{2,1,0:T(8,128)(2,1)S(1)}, bf16[1,2048,512]{2,1,0:T(8,128)(2,1)}, u32[]{:S(2)}) copy-start(bf16[1,2048,512]{2,1,0:T(8,128)(2,1)} %param.20) | copy-start | bytes 6291460
  101.5 5.0 %copy-start.11 = (bf16[16,48,2048]{2,1,0:T(8,128)(2,1)S(1)}, bf16[16,48,2048]{2,1,0:T(8,128)(2,1)}, u32[]{:S(2)}) copy-start(bf16[16,48,2048]{2,1,0:T(8,128)(2,1)} %all-gather.6.cloned.1.call-done) | copy-start | bytes 9437188
  117.8 6.4 %copy-start.3 = (bf16[768,512]{1,0:T(8,128)(2,1)}, bf16[768,512]{1,0:T(8,128)(2,1)S(1)}, u32[]{:S(2)}) copy-start(bf16[768,512]{1,0:T(8,128)(2,1)S(1)} %get-tuple-element.19) | copy-start | bytes 2359300
  117.8 1.9 copy-start.6
  120.7 3.5 %collective-permute-start = (bf16[768,1024]{1,0:T(8,128)(2,1)S(1)}, bf16[768,1024]{1,0:T(8,128)(2,1)S(1)}, u32[]{:S(2)}, u32[]{:S(2)}) collective-permute-start(bf16[768,1024]{1,0:T(8,128)(2,1)S(1)} %add_convert_fusion.1), channel_id=1, source_target_pairs={{0,1},{1,0},{2,3},{3,2},{4,5},{5,4},{6,7},{7,6},{8,9},{9,8},{10,11... | collective-permute-start | bytes 4718600 | tf_op jit(solution)/shard_map/ppermute | solution.py:23
  126.3 7.2 %copy-start.2 = (bf16[192,1024]{1,0:T(8,128)(2,1)S(1)}, bf16[192,1024]{1,0:T(8,128)(2,1)}, u32[]{:S(2)}) copy-start(bf16[192,1024]{1,0:T(8,128)(2,1)} %prev_ref.1) | copy-start | bytes 1179652
  126.3 7.2 %copy-start.7 = (bf16[192,1024]{1,0:T(8,128)(2,1)S(1)}, bf16[192,1024]{1,0:T(8,128)(2,1)}, u32[]{:S(2)}) copy-start(bf16[192,1024]{1,0:T(8,128)(2,1)} %pre_ref.1) | copy-start | bytes 1179652
  126.3 41.2 %all-to-all-start.2 = ((bf16[16,48,1024]{2,1,0:T(8,128)(2,1)}), bf16[16,48,1024]{2,1,0:T(8,128)(2,1)S(1)}, u32[]{:S(2)}, u32[]{:S(2)}) async-start(bf16[16,48,1024]{2,1,0:T(8,128)(2,1)} %bitcast.22), calls=%async_computation.2 | async-start | bytes 3145728 | tf_op jit(solution)/shard_map/all_to_all | solution.py:233
  133.3 45.7 %all-gather.10.cloned.1.call-start = ((), (), s32[]{:S(2)}) async-start(), calls=%async_computation.7 | async-start | bytes 1966080 | tf_op jit(solution)/shard_map/all_gather | solution.py:207
  169.2 1.8 collective-permute-start.1
  172.3 15.7 %all-to-all-start.3 = ((bf16[4,192,512]{2,1,0:T(8,128)(2,1)}), bf16[4,192,512]{2,1,0:T(8,128)(2,1)S(1)}, u32[]{:S(2)}, u32[]{:S(2)}) async-start(bf16[4,192,512]{2,1,0:T(8,128)(2,1)} %pad_maximum_fusion), calls=%async_computation.3 | async-start | bytes 1572864 | tf_op jit(solution)/shard_map/all_to_all | solution.py:260
  176.7 87.2 %reduce-scatter.2.cloned.1.call-start = ((), (), s32[]{:S(2)}) async-start(), calls=%async_computation.8 | async-start | bytes 1310720 | tf_op jit(solution)/shard_map/reduce_scatter | solution.py:265
  188.0 0.9 copy-start.8
  188.9 7.1 %copy-start.4 = (bf16[768,512]{1,0:T(8,128)(2,1)S(1)}, bf16[768,512]{1,0:T(8,128)(2,1)}, u32[]{:S(2)}) copy-start(bf16[768,512]{1,0:T(8,128)(2,1)} %copy-done.3) | copy-start | bytes 2359300
  192.6 66.7 %collective-permute-start.2 = (bf16[1,1024]{1,0:T(2,128)(2,1)S(1)}, bf16[1,1024]{1,0:T(2,128)(2,1)S(1)}, u32[]{:S(2)}, u32[]{:S(2)}) collective-permute-start(bf16[1,1024]{1,0:T(2,128)(2,1)S(1)} %slice.83), channel_id=1, source_target_pairs={{0,2},{2,4},{4,6},{6,8},{8,10},{10,12},{12,14},{14,16},{16,18},{18... | collective-permute-start | bytes 6152 | tf_op jit(solution)/shard_map/ppermute | solution.py:19
  196.0 5.9 %copy-start.12 = (bf16[16,48,2048]{2,1,0:T(8,128)(2,1)S(1)}, bf16[16,48,2048]{2,1,0:T(8,128)(2,1)}, u32[]{:S(2)}) copy-start(bf16[16,48,2048]{2,1,0:T(8,128)(2,1)} %all-gather.6.cloned.1.call-done) | copy-start | bytes 9437188
  201.9 3.9 %copy-start.13 = (bf16[16,48,2048]{2,1,0:T(8,128)(2,1)S(1)}, bf16[16,48,2048]{2,1,0:T(8,128)(2,1)}, u32[]{:S(2)}) copy-start(bf16[16,48,2048]{2,1,0:T(8,128)(2,1)} %all-gather.8.cloned.1.call-done) | copy-start | bytes 9437188
  201.9 3.9 %copy-start.14 = (f32[768,512]{1,0:T(8,128)S(1)}, f32[768,512]{1,0:T(8,128)}, u32[]{:S(2)}) copy-start(f32[768,512]{1,0:T(8,128)} %fusion) | copy-start | bytes 4718596
  201.9 3.9 %copy-start.15 = (f32[768,512]{1,0:T(8,128)S(1)}, f32[768,512]{1,0:T(8,128)}, u32[]{:S(2)}) copy-start(f32[768,512]{1,0:T(8,128)} %fusion.2) | copy-start | bytes 4718596
  210.7 55.0 %copy-start.1 = (bf16[1,2048,512]{2,1,0:T(8,128)(2,1)S(1)}, bf16[1,2048,512]{2,1,0:T(8,128)(2,1)}, u32[]{:S(2)}) copy-start(bf16[1,2048,512]{2,1,0:T(8,128)(2,1)} %param.19) | copy-start | bytes 6291460
  259.3 0.6 copy-start.9
Sparse Core Ops, SparseCore 0:
  55.7 14.2 all-gather.5
  101.6 10.4 all-gather.7
Sparse Core Ops, SparseCore 1:
  136.2 42.7 all-gather.9
  192.7 28.9 reduce-scatter.1

commit v2 on v1

--- a/solution.py
+++ b/solution.py
@@ -137,6 +137,50 @@
             flops=8 * rows * width, bytes_accessed=5 << 20, transcendentals=0
         ),
     )(mine, edges, grad, coef, log_decay, lru_out, before_row)
+
+
+def spread_kernel(count, edge_ref, out_ref, send_sems, recv_sems):
+    mine = lax.axis_index("sp")
+    barrier = pltpu.get_barrier_semaphore()
+    for step in range(1, count):
+        pl.semaphore_signal(
+            barrier,
+            inc=1,
+            device_id={"sp": lax.rem(mine + step, count)},
+            device_id_type=pl.DeviceIdType.MESH,
+        )
+    out_ref[mine] = edge_ref[...]
+    pl.semaphore_wait(barrier, count - 1)
+    copies = []
+    for step in range(1, count):
+        copy = pltpu.make_async_remote_copy(
+            src_ref=edge_ref,
+            dst_ref=out_ref.at[mine],
+            send_sem=send_sems.at[step - 1],
+            recv_sem=recv_sems.at[step - 1],
+            device_id={"sp": lax.rem(mine + step, count)},
+            device_id_type=pl.DeviceIdType.MESH,
+        )
+        copy.start()
+        copies.append(copy)
+    for copy in copies:
+        copy.wait()
+
+
+def spread_edges(edge):
+    count = lax.axis_size("sp")
+    return pl.pallas_call(
+        functools.partial(spread_kernel, count),
+        out_shape=jax.ShapeDtypeStruct((count,) + edge.shape, edge.dtype),
+        in_specs=[pl.BlockSpec(memory_space=pltpu.VMEM)],
+        out_specs=pl.BlockSpec(memory_space=pltpu.VMEM),
+        scratch_shapes=[
+            pltpu.SemaphoreType.DMA((count - 1,)),
+            pltpu.SemaphoreType.DMA((count - 1,)),
+        ],
+        compiler_params=pltpu.CompilerParams(collective_id=0, has_side_effects=True),
+        cost_estimate=pl.CostEstimate(flops=0, bytes_accessed=16 << 20, transcendentals=0),
+    )(edge)
 
 
 def on_device(
@@ -267,7 +311,7 @@
     ).astype(jnp.float32)
 
     d_gate, local_grad, coef, edge = local_part(d_mid, w_out, gate_pre, lru_out, log_decay)
-    edges = lax.all_gather(edge, "sp")
+    edges = spread_edges(edge)
     mine = lax.axis_index("sp").reshape(1).astype(jnp.int32)
     d_drive, d_log_decay = finish_part(
         mine, edges, local_grad, coef, log_decay, lru_out, before_row

time: 274 us -> 244 us (0.89)
  blocking collectives: 86.1 us -> 44.5 us
  Pallas kernels: 11 us -> 22.6 us
    all_gather x1 -> x0, blocking collectives: 41.6 us -> none  [on_device(): edges = lax.all_gather(edge, 'sp')]
    pallas_call x0 -> x1, Pallas kernels: none -> 11.6 us  [spread_edges(): pl.pallas_call(functools.partial(spread_kernel, count), out_shape=jax.Sha...]
  transfers between devices with their start and end apart: 10 -> 10, of which waited for: 7 -> 7; matrix products, arithmetic and copies ran while one was open for 11% -> 12% of each run, Pallas kernels for 4% -> 9%
where the time goes in v2:
time: 244 us; the launch traced here: 243 us
  waiting for transfers between devices  83.6 us (34%)
  blocking collectives  44.5 us (18%)
  matrix products  42.2 us (17%)
  starting transfers between devices  23.8 us (10%)
  Pallas kernels  22.6 us (9%)
  between operations  15.8 us (6%)
  other arithmetic  7.27 us (3%)
  local copies, waits for them, and re-layouts  3.38 us (1%)
    all_to_all x1, blocking collectives, on_device(): lax.all_to_all(cot_piece, 'sp', split_axis=0, concat_axis=0, tiled=True)  44.5 us
    all_to_all x1, waiting for transfers between devices, on_device(): lax.all_to_all(summed_back, 'sp', split_axis=0, concat_axis=0, tiled=True)  32.9 us
    all_to_all x1, waiting for transfers between devices, on_device(): lax.all_to_all(rows_piece, 'sp', split_axis=0, concat_axis=0, tiled=True)  32.9 us
    dot_general x6, matrix products, contract_rows(): lax.dot_general(left, right, (((0,), (0,)), ((), ())), preferred_element_...  21.4 us
    pallas_call x1, Pallas kernels, spread_edges(): pl.pallas_call(functools.partial(spread_kernel, count), out_shape=jax.Sha...  11.6 us
    dot_general x5, matrix products, contract_cols(): lax.dot_general(left, right, (((1,), (1,)), ((), ())), preferred_element_...  10.9 us
    dot_general x5, matrix products, dot(): return jnp.dot(left, right, preferred_element_type=jnp.float32)  9.86 us
    all_to_all x1, waiting for transfers between devices, on_device(): lax.all_to_all(mid_pieces, 'sp', split_axis=0, concat_axis=0, tiled=True,...  9 us
  transfers between devices with their start and end apart: 10, of which 7 were waited for; matrix products, arithmetic and copies ran while one was open for 12% of the time, Pallas kernels for 9%

profile of v2, /device:TPU:0, one launch (start us, length us, event | category | flops | bytes accessed | tf_op | source)
XLA Modules:
  0.0 243.2 jit_solution(2593173875196799096)
XLA Ops:
  8.0 0.0 copy-start
  8.0 0.9 fusion.56
  8.9 0.1 convert_reduce_fusion
  9.0 0.2 fusion.12
  9.2 0.2 fusion.13
  9.4 0.8 multiply_add_fusion
  10.1 2.9 %convolution_convert_fusion = bf16[768,1024]{1,0:T(8,128)(2,1)} fusion(bf16[192,2048]{1,0:T(8,128)(2,1)} %param.11, s32[]{:T(128)S(6)} %select_n.22, s32[192]{0:T(256)S(1)} %bitcast.75, s32[192]{0:T(256)S(1)} %bitcast.72), kind=kOutput, calls=%fused_computation.12 | convolution fusion | flops 303218688 | bytes 1967620 | tf_op jit(solution)/shard_map/dot_general | solution.py:27
  13.0 8.4 %all-to-all-start = ((bf16[16,48,1024]{2,1,0:T(8,128)(2,1)}), bf16[16,48,1024]{2,1,0:T(8,128)(2,1)}, u32[]{:S(2)}, u32[]{:S(2)}) async-start(bf16[16,48,1024]{2,1,0:T(8,128)(2,1)} %bitcast.68), calls=%async_computation | async-start | bytes 3145728 | tf_op jit(solution)/shard_map/all_to_all | solution.py:244
  21.4 0.0 all-gather.4.cloned.1.call-start
  21.5 0.0 copy-done.10
  21.5 1.2 fusion.24
  22.7 32.9 %all-to-all-done = bf16[16,48,1024]{2,1,0:T(8,128)(2,1)} async-done(((bf16[16,48,1024]{2,1,0:T(8,128)(2,1)}), bf16[16,48,1024]{2,1,0:T(8,128)(2,1)}, u32[]{:S(2)}, u32[]{:S(2)}) %all-to-all-start) | async-done | bytes 1572896 | tf_op jit(solution)/shard_map/all_to_all | solution.py:244
  55.6 0.0 all-gather.4.cloned.1.call-update
  55.6 0.0 all-gather.6.cloned.1.call-start
  55.7 0.2 iota_compare_fusion
  55.9 1.0 convolution_convert_fusion.1
  56.9 44.5 %all_to_all.20 = bf16[16,48,1024]{2,1,0:T(8,128)(2,1)} all-to-all(bf16[16,48,1024]{2,1,0:T(8,128)(2,1)S(1)} %bitcast.70), channel_id=1, replica_groups=mesh['sp'=16,'tp'=2] {'sp'}, dimensions={0} | all-to-all | bytes 3145728 | tf_op jit(solution)/shard_map/all_to_all | solution.py:245
  101.5 0.0 all-gather.6.cloned.1.call-update
  101.5 0.0 all-gather.4.cloned.1.call-done
  101.5 0.0 copy-done
  101.5 0.0 copy-start.5
  101.5 5.0 %fusion = f32[768,512]{1,0:T(8,128)} fusion(bf16[768,2048]{1,0:T(8,128)(2,1)} %bitcast.85, bf16[1,2048,512]{2,1,0:T(8,128)(2,1)S(1)} %copy-done), kind=kOutput, calls=%fused_computation.6 | convolution fusion | flops 1610612736 | bytes 6815744 | tf_op jit(solution)/shard_map/dot_general | solution.py:39
  106.5 2.9 %fusion.2 = f32[768,512]{1,0:T(8,128)} fusion(bf16[768,2048]{1,0:T(8,128)(2,1)S(1)} %bitcast.87, bf16[1,2048,512]{2,1,0:T(8,128)(2,1)S(1)} %copy-done.5), kind=kOutput, calls=%fused_computation.8 | convolution fusion | flops 1610612736 | bytes 6815744 | tf_op jit(solution)/shard_map/dot_general | solution.py:39
  109.4 2.6 %all-gather.6.cloned.1.call-done = bf16[16,48,2048]{2,1,0:T(8,128)(2,1)} async-done(((bf16[16,48,1024]{2,1,0:T(8,128)(2,1)}), bf16[16,48,2048]{2,1,0:T(8,128)(2,1)}) %all-gather.6.cloned.1.call-update) | async-done | bytes 3145744 | tf_op jit(solution)/shard_map/all_gather | solution.py:247
  112.1 5.7 %multiply_convert_fusion.1 = (bf16[768,512]{1,0:T(8,128)(2,1)S(1)}, bf16[768,512]{1,0:T(8,128)(2,1)S(1)}) fusion(f32[768,512]{1,0:T(8,128)} %fusion, f32[768,512]{1,0:T(8,128)} %fusion.2, bf16[768,2048]{1,0:T(8,128)(2,1)} %bitcast.89, bf16[1,512,2048]{2,1,0:T(8,128)(2,1)} %param.21), kind=kOutput, calls=%fused_computation.15 | convolution fusion | flops 1615724544 | bytes 9961472 | tf_op jit(solution)/shard_map/dot_general | solution.py:33
  117.8 0.0 copy-start.3
  117.8 0.0 copy-start.6
  117.8 1.0 fusion.15
  118.8 0.8 copy-done.6
  119.7 1.0 add_convert_fusion.1
  120.7 0.3 collective-permute-start
  121.0 1.0 fusion.18
  122.0 2.2 collective-permute-done
  124.2 2.2 add_convert_fusion
  126.3 6.9 %all-to-all-start.2 = ((bf16[16,48,1024]{2,1,0:T(8,128)(2,1)}), bf16[16,48,1024]{2,1,0:T(8,128)(2,1)S(1)}, u32[]{:S(2)}, u32[]{:S(2)}) async-start(bf16[16,48,1024]{2,1,0:T(8,128)(2,1)} %bitcast.22), calls=%async_computation.2 | async-start | bytes 3145728 | tf_op jit(solution)/shard_map/all_to_all | solution.py:277
  133.3 0.2 all-gather.8.cloned.1.call-start
  133.5 1.1 fusion.32
  134.6 0.0 all-gather.8.cloned.1.call-update
  134.6 32.9 %all-to-all-done.2 = bf16[16,48,1024]{2,1,0:T(8,128)(2,1)S(1)} async-done(((bf16[16,48,1024]{2,1,0:T(8,128)(2,1)}), bf16[16,48,1024]{2,1,0:T(8,128)(2,1)S(1)}, u32[]{:S(2)}, u32[]{:S(2)}) %all-to-all-start.2) | async-done | bytes 1572896 | tf_op jit(solution)/shard_map/all_to_all | solution.py:277
  167.6 1.6 fusion.7
  169.2 0.1 collective-permute-start.1
  169.3 1.7 collective-permute-done.1
  171.0 0.1 broadcast_select_fusion.1
  171.0 0.1 fusion.53
  171.1 0.1 fusion.54
  171.3 1.0 pad_maximum_fusion
  172.3 4.4 %all-to-all-start.3 = ((bf16[4,192,512]{2,1,0:T(8,128)(2,1)}), bf16[4,192,512]{2,1,0:T(8,128)(2,1)S(1)}, u32[]{:S(2)}, u32[]{:S(2)}) async-start(bf16[4,192,512]{2,1,0:T(8,128)(2,1)} %pad_maximum_fusion), calls=%async_computation.3 | async-start | bytes 1572864 | tf_op jit(solution)/shard_map/all_to_all | solution.py:304
  176.7 2.2 all-gather.8.cloned.1.call-done
  179.0 9.0 %all-to-all-done.3 = bf16[4,192,512]{2,1,0:T(8,128)(2,1)S(1)} async-done(((bf16[4,192,512]{2,1,0:T(8,128)(2,1)}), bf16[4,192,512]{2,1,0:T(8,128)(2,1)S(1)}, u32[]{:S(2)}, u32[]{:S(2)}) %all-to-all-start.3) | async-done | bytes 786464 | tf_op jit(solution)/shard_map/all_to_all | solution.py:304
  188.0 0.9 copy-done.8
  188.9 3.7 %convolution_convert_fusion.2 = bf16[512,1024]{1,0:T(8,128)(2,1)} fusion(bf16[768,512]{1,0:T(8,128)(2,1)} %bitcast.71, bf16[768,1024]{1,0:T(8,128)(2,1)} %all-gather.8.cloned.1.call-done), kind=kOutput, calls=%fused_computation.19 | convolution fusion | flops 805830656 | bytes 3407872 | tf_op jit(solution)/shard_map/dot_general | solution.py:27
  192.6 0.0 reduce-scatter.2.cloned.1.call-update
  192.6 3.4 %collective-permute-start.2 = (bf16[1,1024]{1,0:T(2,128)(2,1)S(1)}, bf16[1,1024]{1,0:T(2,128)(2,1)S(1)}, u32[]{:S(2)}, u32[]{:S(2)}) collective-permute-start(bf16[1,1024]{1,0:T(2,128)(2,1)S(1)} %slice.83), channel_id=1, source_target_pairs={{0,2},{2,4},{4,6},{6,8},{8,10},{10,12},{12,14},{14,16},{16,18},{18... | collective-permute-start | bytes 6152 | tf_op jit(solution)/shard_map/ppermute | solution.py:19
  196.0 5.9 %convolution_bitcast_fusion.1 = f32[1,2048,512]{2,1,0:T(8,128)} fusion(bf16[768,2048]{1,0:T(8,128)(2,1)} %bitcast.86, bf16[768,512]{1,0:T(8,128)(2,1)S(1)} %copy-done.4), kind=kOutput, calls=%fused_computation.1 | convolution fusion | flops 1610612736 | bytes 8126464 | tf_op jit(solution)/shard_map/dot_general | solution.py:27
  201.9 3.9 %convolution_bitcast_fusion.2 = f32[1,2048,512]{2,1,0:T(8,128)} fusion(bf16[768,2048]{1,0:T(8,128)(2,1)S(1)} %bitcast.88, bf16[768,512]{1,0:T(8,128)(2,1)S(1)} %get-tuple-element.20), kind=kOutput, calls=%fused_computation.2 | convolution fusion | flops 1610612736 | bytes 8126464 | tf_op jit(solution)/shard_map/dot_general | solution.py:27
  205.8 4.0 %convolution_bitcast_fusion = f32[1,512,2048]{2,1,0:T(8,128)} fusion(bf16[768,2048]{1,0:T(8,128)(2,1)S(1)} %bitcast.90, f32[768,512]{1,0:T(8,128)S(1)} %copy-done.15, f32[768,512]{1,0:T(8,128)S(1)} %copy-done.14), kind=kOutput, calls=%fused_computation | convolution fusion | flops 1612972032 | bytes 10485760 | tf_op jit(solution)/shard_map/dot_general | solution.py:27
  209.8 0.9 pad_maximum_fusion.1.mid_ref
  210.7 7.0 %shard_map.162 = (bf16[192,1024]{1,0:T(8,128)(2,1)}, f32[192,1024]{1,0:T(8,128)}, f32[192,1024]{1,0:T(8,128)}, f32[2,1024]{1,0:T(2,128)}) custom-call(bf16[192,2048]{1,0:T(8,128)(2,1)} %pad_maximum_fusion.1.mid_ref, bf16[1024,2048]{1,0:T(8,128)(2,1)} %w_ref.1, bf16[192,1024]{1,0:T(8,128)(2,1)} %pre_ref.1, bf16[192,1024]{1,0:T(8,128)(2,1)} %prev_ref.1, ...), custom_call_target="tpu_custom_call" | custom-call | flops 805306368 | bytes 8388608 | tf_op jit(solution)/shard_map/pallas_call | solution.py:80
  217.8 11.6 %shard_map.163.edges_ref = f32[16,2,1024]{2,1,0:T(2,128)} custom-call(f32[2,1024]{1,0:T(2,128)} %get-tuple-element.14.edge_ref), custom_call_target="tpu_custom_call" | custom-call | bytes 16777216 | tf_op jit(solution)/shard_map/pallas_call | solution.py:172
  229.4 0.0 collective-permute-done.2.before_ref
  229.4 0.0 copy-start.9
  229.4 0.6 copy-done.9
  230.0 4.0 %shard_map.164 = (f32[192,1024]{1,0:T(8,128)}, f32[192,1024]{1,0:T(8,128)}) custom-call(s32[1]{0:T(128)} %bitcast.29.mine_ref, f32[16,2,1024]{2,1,0:T(2,128)} %shard_map.163.edges_ref, f32[192,1024]{1,0:T(8,128)} %get-tuple-element.15.grad_ref, f32[192,1024]{1,0:T(8,128)} %get-tuple-element.16.coef_ref, f32[192,1024]{1,0:T(8,128)} %log_ref.3, ...), custom_call_target="tpu_custom_call" | custom-call | flops 1572864 | bytes 5242880 | tf_op jit(solution)/shard_map/pallas_call | solution.py:122
  234.0 1.8 convert_element_type.127
  (32 shorter events, 0.2 us)
Async XLA Ops:
  8.0 93.5 %copy-start = (bf16[1,2048,512]{2,1,0:T(8,128)(2,1)S(1)}, bf16[1,2048,512]{2,1,0:T(8,128)(2,1)}, u32[]{:S(2)}) copy-start(bf16[1,2048,512]{2,1,0:T(8,128)(2,1)} %param.19) | copy-start | bytes 6291460
  10.1 11.3 %copy-start.10 = (f32[192,2]{0,1:T(2,128)S(1)}, f32[192,2]{0,1:T(2,128)}, u32[]{:S(2)}) copy-start(f32[192,2]{0,1:T(2,128)} %param.14) | copy-start | bytes 4612
  13.0 42.6 %all-to-all-start = ((bf16[16,48,1024]{2,1,0:T(8,128)(2,1)}), bf16[16,48,1024]{2,1,0:T(8,128)(2,1)}, u32[]{:S(2)}, u32[]{:S(2)}) async-start(bf16[16,48,1024]{2,1,0:T(8,128)(2,1)} %bitcast.68), calls=%async_computation | async-start | bytes 3145728 | tf_op jit(solution)/shard_map/all_to_all | solution.py:244
  21.4 80.1 %all-gather.4.cloned.1.call-start = ((), (), s32[]{:S(2)}) async-start(), calls=%async_computation.5 | async-start | bytes 4718592 | tf_op jit(solution)/shard_map/all_gather | solution.py:246
  55.6 56.5 %all-gather.6.cloned.1.call-start = ((), (), s32[]{:S(2)}) async-start(), calls=%async_computation.6 | async-start | bytes 4718592 | tf_op jit(solution)/shard_map/all_gather | solution.py:247
  101.5 5.0 %copy-start.5 = (bf16[1,2048,512]{2,1,0:T(8,128)(2,1)S(1)}, bf16[1,2048,512]{2,1,0:T(8,128)(2,1)}, u32[]{:S(2)}) copy-start(bf16[1,2048,512]{2,1,0:T(8,128)(2,1)} %param.20) | copy-start | bytes 6291460
  101.5 5.0 %copy-start.11 = (bf16[16,48,2048]{2,1,0:T(8,128)(2,1)S(1)}, bf16[16,48,2048]{2,1,0:T(8,128)(2,1)}, u32[]{:S(2)}) copy-start(bf16[16,48,2048]{2,1,0:T(8,128)(2,1)} %all-gather.4.cloned.1.call-done) | copy-start | bytes 9437188
  117.8 6.4 %copy-start.3 = (bf16[768,512]{1,0:T(8,128)(2,1)}, bf16[768,512]{1,0:T(8,128)(2,1)S(1)}, u32[]{:S(2)}) copy-start(bf16[768,512]{1,0:T(8,128)(2,1)S(1)} %get-tuple-element.19) | copy-start | bytes 2359300
  117.8 1.9 copy-start.6
  120.7 3.5 %collective-permute-start = (bf16[768,1024]{1,0:T(8,128)(2,1)S(1)}, bf16[768,1024]{1,0:T(8,128)(2,1)S(1)}, u32[]{:S(2)}, u32[]{:S(2)}) collective-permute-start(bf16[768,1024]{1,0:T(8,128)(2,1)S(1)} %add_convert_fusion.1), channel_id=1, source_target_pairs={{0,1},{1,0},{2,3},{3,2},{4,5},{5,4},{6,7},{7,6},{8,9},{9,8},{10,11... | collective-permute-start | bytes 4718600 | tf_op jit(solution)/shard_map/ppermute | solution.py:23
  126.3 7.2 %copy-start.2 = (bf16[192,1024]{1,0:T(8,128)(2,1)S(1)}, bf16[192,1024]{1,0:T(8,128)(2,1)}, u32[]{:S(2)}) copy-start(bf16[192,1024]{1,0:T(8,128)(2,1)} %prev_ref.1) | copy-start | bytes 1179652
  126.3 7.2 %copy-start.7 = (bf16[192,1024]{1,0:T(8,128)(2,1)S(1)}, bf16[192,1024]{1,0:T(8,128)(2,1)}, u32[]{:S(2)}) copy-start(bf16[192,1024]{1,0:T(8,128)(2,1)} %pre_ref.1) | copy-start | bytes 1179652
  126.3 41.2 %all-to-all-start.2 = ((bf16[16,48,1024]{2,1,0:T(8,128)(2,1)}), bf16[16,48,1024]{2,1,0:T(8,128)(2,1)S(1)}, u32[]{:S(2)}, u32[]{:S(2)}) async-start(bf16[16,48,1024]{2,1,0:T(8,128)(2,1)} %bitcast.22), calls=%async_computation.2 | async-start | bytes 3145728 | tf_op jit(solution)/shard_map/all_to_all | solution.py:277
  133.3 45.7 %all-gather.8.cloned.1.call-start = ((), (), s32[]{:S(2)}) async-start(), calls=%async_computation.7 | async-start | bytes 1966080 | tf_op jit(solution)/shard_map/all_gather | solution.py:251
  169.2 1.8 collective-permute-start.1
  172.3 15.7 %all-to-all-start.3 = ((bf16[4,192,512]{2,1,0:T(8,128)(2,1)}), bf16[4,192,512]{2,1,0:T(8,128)(2,1)S(1)}, u32[]{:S(2)}, u32[]{:S(2)}) async-start(bf16[4,192,512]{2,1,0:T(8,128)(2,1)} %pad_maximum_fusion), calls=%async_computation.3 | async-start | bytes 1572864 | tf_op jit(solution)/shard_map/all_to_all | solution.py:304
  176.7 57.3 %reduce-scatter.2.cloned.1.call-start = ((), (), s32[]{:S(2)}) async-start(), calls=%async_computation.8 | async-start | bytes 1310720 | tf_op jit(solution)/shard_map/reduce_scatter | solution.py:309
  188.0 0.9 copy-start.8
  188.9 7.1 %copy-start.4 = (bf16[768,512]{1,0:T(8,128)(2,1)S(1)}, bf16[768,512]{1,0:T(8,128)(2,1)}, u32[]{:S(2)}) copy-start(bf16[768,512]{1,0:T(8,128)(2,1)} %copy-done.3) | copy-start | bytes 2359300
  192.6 36.8 %collective-permute-start.2 = (bf16[1,1024]{1,0:T(2,128)(2,1)S(1)}, bf16[1,1024]{1,0:T(2,128)(2,1)S(1)}, u32[]{:S(2)}, u32[]{:S(2)}) collective-permute-start(bf16[1,1024]{1,0:T(2,128)(2,1)S(1)} %slice.83), channel_id=1, source_target_pairs={{0,2},{2,4},{4,6},{6,8},{8,10},{10,12},{12,14},{14,16},{16,18},{18... | collective-permute-start | bytes 6152 | tf_op jit(solution)/shard_map/ppermute | solution.py:19
  196.0 5.9 %copy-start.12 = (bf16[16,48,2048]{2,1,0:T(8,128)(2,1)S(1)}, bf16[16,48,2048]{2,1,0:T(8,128)(2,1)}, u32[]{:S(2)}) copy-start(bf16[16,48,2048]{2,1,0:T(8,128)(2,1)} %all-gather.4.cloned.1.call-done) | copy-start | bytes 9437188
  201.9 3.9 %copy-start.13 = (bf16[16,48,2048]{2,1,0:T(8,128)(2,1)S(1)}, bf16[16,48,2048]{2,1,0:T(8,128)(2,1)}, u32[]{:S(2)}) copy-start(bf16[16,48,2048]{2,1,0:T(8,128)(2,1)} %all-gather.6.cloned.1.call-done) | copy-start | bytes 9437188
  201.9 3.9 %copy-start.14 = (f32[768,512]{1,0:T(8,128)S(1)}, f32[768,512]{1,0:T(8,128)}, u32[]{:S(2)}) copy-start(f32[768,512]{1,0:T(8,128)} %fusion) | copy-start | bytes 4718596
  201.9 3.9 %copy-start.15 = (f32[768,512]{1,0:T(8,128)S(1)}, f32[768,512]{1,0:T(8,128)}, u32[]{:S(2)}) copy-start(f32[768,512]{1,0:T(8,128)} %fusion.2) | copy-start | bytes 4718596
  210.7 25.1 %copy-start.1 = (bf16[1,2048,512]{2,1,0:T(8,128)(2,1)S(1)}, bf16[1,2048,512]{2,1,0:T(8,128)(2,1)}, u32[]{:S(2)}) copy-start(bf16[1,2048,512]{2,1,0:T(8,128)(2,1)} %param.19) | copy-start | bytes 6291460
  229.4 0.6 copy-start.9
Sparse Core Ops, SparseCore 0:
  55.7 14.2 all-gather.3
  101.6 10.4 all-gather.5
Sparse Core Ops, SparseCore 1:
  136.2 42.7 all-gather.7
  192.7 28.9 reduce-scatter.1

commit v3 on v2

--- a/solution.py
+++ b/solution.py
@@ -226,23 +226,55 @@
         place = jnp.sum(rank * wide, axis=1, keepdims=True).astype(jnp.int32)
         hits.append(slots == chosen * capacity + place)
     any_hit = (hits[0] | hits[1]).astype(jnp.bfloat16)
-    each_hit = jnp.concatenate([hit.astype(jnp.bfloat16) for hit in hits], axis=0)
     stream_half = lax.dynamic_slice_in_dim(stream_mid, own_start, half_cols, 1)
     cot_half = lax.dynamic_slice_in_dim(d_out, own_start, half_cols, 1)
     cot_wide = cot_half.astype(jnp.float32)
-    scaled = jnp.concatenate(
-        [
-            (route_weights[:, pick : pick + 1] * cot_wide).astype(jnp.bfloat16)
-            for pick in range(TOPK)
-        ],
-        axis=0,
-    )
-    rows_piece = contract_rows(any_hit, stream_half).astype(jnp.bfloat16)
-    cot_piece = contract_rows(each_hit, scaled).astype(jnp.bfloat16)
-    rows_piece = rows_piece.reshape(sp_count, EXP_DEV * capacity, half_cols)
-    cot_piece = cot_piece.reshape(sp_count, EXP_DEV * capacity, half_cols)
-    got_rows = lax.all_to_all(rows_piece, "sp", split_axis=0, concat_axis=0, tiled=True)
-    got_cot = lax.all_to_all(cot_piece, "sp", split_axis=0, concat_axis=0, tiled=True)
+
+    def line_gather(value):
+        return lax.all_gather(value, "sp", axis=0, tiled=True, axis_index_groups=line_groups)
+
+    line_stream = line_gather(stream_half)
+    line_cot = line_gather(cot_half)
+    routes = line_gather(jnp.concatenate([route_ids.astype(jnp.float32), route_weights], axis=1))
+    plane_start = lax.axis_index("sp") // plane * plane
+    locals_ = jnp.arange(plane, dtype=jnp.int32)[None, :]
+    plane_slots = jnp.arange(plane * capacity, dtype=jnp.int32)[None, :]
+    row_blocks, cot_blocks = ([], [])
+    for line in range(lines):
+        block = slice(line * rows_local, (line + 1) * rows_local)
+        block_cot = line_cot[block].astype(jnp.float32)
+        block_hits, block_scaled = ([], [])
+        before = jnp.zeros((1, plane), jnp.float32)
+        for pick in range(TOPK):
+            chosen = routes[block, pick : pick + 1].astype(jnp.int32) - plane_start
+            onehot = (chosen == locals_).astype(jnp.bfloat16)
+            wide = onehot.astype(jnp.float32)
+            rank = dot(earlier, onehot) + before
+            before = before + jnp.sum(wide, axis=0, keepdims=True)
+            place = jnp.sum(rank * wide, axis=1, keepdims=True).astype(jnp.int32)
+            block_hits.append(plane_slots == chosen * capacity + place)
+            weight = routes[block, TOPK + pick : TOPK + pick + 1]
+            block_scaled.append((weight * block_cot).astype(jnp.bfloat16))
+        block_any = (block_hits[0] | block_hits[1]).astype(jnp.bfloat16)
+        block_each = jnp.concatenate([hit.astype(jnp.bfloat16) for hit in block_hits], axis=0)
+        shape = (plane, 1, capacity, half_cols)
+        row_blocks.append(
+            contract_rows(block_any, line_stream[block]).astype(jnp.bfloat16).reshape(shape)
+        )
+        cot_blocks.append(
+            contract_rows(block_each, jnp.concatenate(block_scaled, axis=0))
+            .astype(jnp.bfloat16)
+            .reshape(shape)
+        )
+
+    def plane_exchange(blocks):
+        pieces = jnp.concatenate(blocks, axis=1).reshape(plane, lines * capacity, half_cols)
+        return lax.all_to_all(
+            pieces, "sp", split_axis=0, concat_axis=0, tiled=True, axis_index_groups=plane_groups
+        )
+
+    got_rows = plane_exchange(row_blocks)
+    got_cot = plane_exchange(cot_blocks)
     inputs = lax.all_gather(got_rows, "tp", axis=2, tiled=True).reshape(slot_count, model_width)
     cotangent = lax.all_gather(got_cot, "tp", axis=2, tiled=True).reshape(slot_count, model_width)
 
@@ -273,8 +305,15 @@
     summed_back = (own_piece.astype(jnp.float32) + from_other.astype(jnp.float32)).astype(
         jnp.bfloat16
     )
+    summed_back = summed_back.reshape(plane, lines, capacity, half_cols).transpose(1, 0, 2, 3)
     summed_back = summed_back.reshape(sp_count, EXP_DEV * capacity, half_cols)
     returned = lax.all_to_all(summed_back, "sp", split_axis=0, concat_axis=0, tiled=True)
+    down_grad = contract_rows(hidden, cotangent)
+    gate_grad = contract_rows(inputs, grad_gate_pre)
+    up_grad = contract_rows(inputs, grad_up_pre)
+    returned, down_grad, gate_grad, up_grad = lax.optimization_barrier(
+        (returned, down_grad, gate_grad, up_grad)
+    )
     routed_back = dot(any_hit, returned.reshape(slot_count, half_cols))
     mid_half = (cot_wide + routed_back).astype(jnp.bfloat16)
     mid_other = swapped(mid_half)
@@ -282,10 +321,6 @@
     d_mid = jnp.concatenate(
         [jnp.where(first, mid_half, mid_other), jnp.where(first, mid_other, mid_half)], axis=1
     )
-
-    down_grad = contract_rows(hidden, cotangent)
-    gate_grad = contract_rows(inputs, grad_gate_pre)
-    up_grad = contract_rows(inputs, grad_up_pre)
 
     share = model_width // sp_count
     mid_pieces = jnp.stack(
@@ -304,13 +339,14 @@
     mid_pieces = lax.all_to_all(
         mid_pieces, "sp", split_axis=0, concat_axis=0, tiled=True, axis_index_groups=plane_groups
     )
+    d_gate, local_grad, coef, edge = local_part(d_mid, w_out, gate_pre, lru_out, log_decay)
+    mid_pieces, edge = lax.optimization_barrier((mid_pieces, edge))
     mid_rows = mid_pieces.reshape(plane * rows_local, lines * share)
     partial = contract_rows(mid_rows, plane_gated).astype(jnp.bfloat16)
     grad_out_proj = lax.psum_scatter(
         partial, "sp", scatter_dimension=0, tiled=True, axis_index_groups=line_groups
     ).astype(jnp.float32)
 
-    d_gate, local_grad, coef, edge = local_part(d_mid, w_out, gate_pre, lru_out, log_decay)
     edges = spread_edges(edge)
     mine = lax.axis_index("sp").reshape(1).astype(jnp.int32)
     d_drive, d_log_decay = finish_part(

time: 244 us -> 247 us (1.012)
  blocking collectives: 44.5 us -> 37.3 us
  waiting for transfers between devices: 83.6 us -> 88.2 us
  local copies, waits for them, and re-layouts: 3.38 us -> 7.54 us
  starting transfers between devices: 23.8 us -> 19.9 us
  other arithmetic: 7.27 us -> 9.94 us
    all_gather x0 -> x2, waiting for transfers between devices: none -> 31 us  [line_gather(): lax.all_gather(value, 'sp', axis=0, tiled=True, axis_index_groups=line_gr...]
    all_to_all x1, blocking collectives: 44.5 us -> 22.4 us  [plane_exchange(): lax.all_to_all(pieces, 'sp', split_axis=0, concat_axis=0, tiled=True, axi...]
    all_gather x0 -> x1, blocking collectives: none -> 14.9 us  [line_gather(): lax.all_gather(value, 'sp', axis=0, tiled=True, axis_index_groups=line_gr...]
    all_to_all x1, waiting for transfers between devices: 32.9 us -> 18.2 us  [plane_exchange(): lax.all_to_all(pieces, 'sp', split_axis=0, concat_axis=0, tiled=True, axi...]
    all_to_all x1, waiting for transfers between devices: 32.9 us -> 18.7 us  [on_device(): lax.all_to_all(summed_back, 'sp', split_axis=0, concat_axis=0, tiled=True)]
    reduce_scatter x1, waiting for transfers between devices: 0.01 us -> 10.2 us  [on_device(): lax.psum_scatter(partial, 'sp', scatter_dimension=0, tiled=True, axis_ind...]
    all_to_all x1, waiting for transfers between devices: 9 us -> 3.41 us  [on_device(): lax.all_to_all(mid_pieces, 'sp', split_axis=0, concat_axis=0, tiled=True,...]
    all_to_all x1, starting transfers between devices: 8.39 us -> 4.38 us  [plane_exchange(): lax.all_to_all(pieces, 'sp', split_axis=0, concat_axis=0, tiled=True, axi...]
  transfers between devices with their start and end apart: 10 -> 12, of which waited for: 7 -> 9; matrix products, arithmetic and copies ran while one was open for 12% -> 17% of each run, Pallas kernels for 9% -> 9%
where the time goes in v3:
time: 247 us; the launch traced here: 246 us
  waiting for transfers between devices  88.2 us (36%)
  matrix products  43.9 us (18%)
  blocking collectives  37.3 us (15%)
  Pallas kernels  23.3 us (9%)
  starting transfers between devices  19.9 us (8%)
  between operations  15.9 us (6%)
  other arithmetic  9.94 us (4%)
  local copies, waits for them, and re-layouts  7.54 us (3%)
    all_gather x2, waiting for transfers between devices, line_gather(): lax.all_gather(value, 'sp', axis=0, tiled=True, axis_index_groups=line_gr...  31 us
    dot_general x12, matrix products, contract_rows(): lax.dot_general(left, right, (((0,), (0,)), ((), ())), preferred_element_...  22.5 us
    all_to_all x1, blocking collectives, plane_exchange(): lax.all_to_all(pieces, 'sp', split_axis=0, concat_axis=0, tiled=True, axi...  22.4 us
    all_to_all x1, waiting for transfers between devices, on_device(): lax.all_to_all(summed_back, 'sp', split_axis=0, concat_axis=0, tiled=True)  18.7 us
    all_to_all x1, waiting for transfers between devices, plane_exchange(): lax.all_to_all(pieces, 'sp', split_axis=0, concat_axis=0, tiled=True, axi...  18.2 us
    all_gather x1, blocking collectives, line_gather(): lax.all_gather(value, 'sp', axis=0, tiled=True, axis_index_groups=line_gr...  14.9 us
    pallas_call x1, Pallas kernels, spread_edges(): pl.pallas_call(functools.partial(spread_kernel, count), out_shape=jax.Sha...  12.4 us
    dot_general x13, matrix products, dot(): return jnp.dot(left, right, preferred_element_type=jnp.float32)  11.6 us
  transfers between devices with their start and end apart: 12, of which 9 were waited for; matrix products, arithmetic and copies ran while one was open for 17% of the time, Pallas kernels for 9%

profile of v3, /device:TPU:0, one launch (start us, length us, event | category | flops | bytes accessed | tf_op | source)
XLA Modules:
  0.0 246.0 jit_solution(3640405803952739711)
XLA Ops:
  8.1 1.9 constant_dynamic-slice_fusion
  10.1 1.8 constant_dynamic-slice_fusion.1
  11.9 14.9 %all-gather = f32[4,192,4]{1,2,0:T(4,128)S(1)} all-gather(f32[1,192,4]{1,2,0:T(4,128)S(1)} %maximum_bitcast_fusion.4), channel_id=1, replica_groups={{0,8,16,24},{2,10,18,26},{4,12,20,28},{6,14,22,30},{1,9,17,25},{3,11,19..., dimensions={0}, use_global_device_ids=true | all-gather | bytes 15360 | tf_op jit(solution)/shard_map/all_gather | solution.py:234
  27.2 0.2 fusion.15
  27.3 0.1 convert_reduce_fusion.3
  27.5 0.2 fusion.17
  27.8 0.2 fusion.19
  28.1 0.2 fusion.21
  28.2 0.2 fusion.16
  28.5 0.2 fusion.18
  28.7 0.2 fusion.20
  28.9 0.2 fusion.22
  29.1 21.7 %all-gather.11.cloned.1.call-done = bf16[768,1024]{1,0:T(8,128)(2,1)} async-done(((bf16[192,1024]{1,0:T(8,128)(2,1)}), bf16[768,1024]{1,0:T(8,128)(2,1)}) %all-gather.11.cloned.1.call-update) | async-done | bytes 1572880 | tf_op jit(solution)/shard_map/all_gather | solution.py:234
  50.8 1.5 convolution_convert_fusion.4
  52.3 1.4 convolution_convert_fusion.3
  53.7 0.4 convolution_convert_fusion.2
  54.1 0.4 convolution_convert_fusion.1
  54.5 1.3 pad_maximum_fusion.1
  55.9 4.4 %all-to-all-start.1 = ((bf16[4,192,1024]{2,1,0:T(8,128)(2,1)}), bf16[4,192,1024]{2,1,0:T(8,128)(2,1)}, u32[]{:S(2)}, u32[]{:S(2)}) async-start(bf16[4,192,1024]{2,1,0:T(8,128)(2,1)} %bitcast.126), calls=%async_computation.1 | async-start | bytes 3145728 | tf_op jit(solution)/shard_map/all_to_all | solution.py:272
  60.7 18.2 %all-to-all-done.1 = bf16[4,192,1024]{2,1,0:T(8,128)(2,1)} async-done(((bf16[4,192,1024]{2,1,0:T(8,128)(2,1)}), bf16[4,192,1024]{2,1,0:T(8,128)(2,1)}, u32[]{:S(2)}, u32[]{:S(2)}) %all-to-all-start.1) | async-done | bytes 1572896 | tf_op jit(solution)/shard_map/all_to_all | solution.py:272
  79.5 9.4 %all-gather.7.cloned.1.call-done = bf16[768,1024]{1,0:T(8,128)(2,1)} async-done(((bf16[192,1024]{1,0:T(8,128)(2,1)}), bf16[768,1024]{1,0:T(8,128)(2,1)}) %all-gather.7.cloned.1.call-update) | async-done | bytes 1572880 | tf_op jit(solution)/shard_map/all_gather | solution.py:234
  88.9 1.9 fusion.33
  90.8 0.4 convolution_convert_fusion.8
  91.2 0.4 convolution_convert_fusion.7
  91.6 0.4 convolution_convert_fusion.6
  92.1 0.4 convolution_convert_fusion.5
  92.5 0.2 pad_maximum_fusion
  92.7 22.4 %all_to_all.20 = bf16[4,192,1024]{2,1,0:T(8,128)(2,1)} all-to-all(bf16[4,192,1024]{2,1,0:T(8,128)(2,1)S(1)} %bitcast.127), channel_id=1, replica_groups={{0,2,4,6},{8,10,12,14},{16,18,20,22},{24,26,28,30},{1,3,5,7},{9,11,13,1..., dimensions={0} | all-to-all | bytes 3145728 | tf_op jit(solution)/shard_map/all_to_all | solution.py:272
  115.1 5.0 %fusion = f32[768,512]{1,0:T(8,128)} fusion(bf16[768,2048]{1,0:T(8,128)(2,1)} %bitcast.189, bf16[1,2048,512]{2,1,0:T(8,128)(2,1)S(1)} %copy-done), kind=kOutput, calls=%fused_computation.3 | convolution fusion | flops 1610612736 | bytes 6815744 | tf_op jit(solution)/shard_map/dot_general | solution.py:39
  120.1 3.0 %fusion.2 = f32[768,512]{1,0:T(8,128)} fusion(bf16[768,2048]{1,0:T(8,128)(2,1)S(1)} %bitcast.191, bf16[1,2048,512]{2,1,0:T(8,128)(2,1)S(1)} %copy-done.5), kind=kOutput, calls=%fused_computation.5 | convolution fusion | flops 1610612736 | bytes 6815744 | tf_op jit(solution)/shard_map/dot_general | solution.py:39
  123.1 2.7 %all-gather.9.cloned.1.call-done = bf16[4,192,2048]{2,1,0:T(8,128)(2,1)} async-done(((bf16[4,192,1024]{2,1,0:T(8,128)(2,1)}), bf16[4,192,2048]{2,1,0:T(8,128)(2,1)}) %all-gather.9.cloned.1.call-update) | async-done | bytes 3145744 | tf_op jit(solution)/shard_map/all_gather | solution.py:279
  125.8 5.7 %multiply_convert_fusion.1 = (bf16[768,512]{1,0:T(8,128)(2,1)S(1)}, bf16[768,512]{1,0:T(8,128)(2,1)S(1)}) fusion(f32[768,512]{1,0:T(8,128)} %fusion, f32[768,512]{1,0:T(8,128)} %fusion.2, bf16[768,2048]{1,0:T(8,128)(2,1)} %bitcast.193, bf16[1,512,2048]{2,1,0:T(8,128)(2,1)} %param.21), kind=kOutput, calls=%fused_computation.12 | convolution fusion | flops 1615724544 | bytes 9961472 | tf_op jit(solution)/shard_map/dot_general | solution.py:33
  131.5 1.0 fusion.24
  132.6 0.8 copy-done.6
  133.4 1.0 add_convert_fusion.1
  134.4 0.3 collective-permute-start
  134.7 1.0 fusion.27
  135.7 2.2 collective-permute-done
  137.9 1.0 add_convert_fusion
  138.9 1.3 copy.37
  140.3 7.0 %all-to-all-start.2 = ((bf16[16,48,1024]{2,1,0:T(8,128)(2,1)}), bf16[16,48,1024]{2,1,0:T(8,128)(2,1)}, u32[]{:S(2)}, u32[]{:S(2)}) async-start(bf16[16,48,1024]{2,1,0:T(8,128)(2,1)} %bitcast.62), calls=%async_computation.2 | async-start | bytes 3145728 | tf_op jit(solution)/shard_map/all_to_all | solution.py:310
  147.2 0.3 all-gather.15.cloned.1.call-start
  147.5 1.1 fusion.47
  148.8 0.2 fusion.10
  149.0 0.2 fusion.9
  149.2 5.9 %fusion.131 = f32[2048,512]{1,0:T(8,128)} fusion(bf16[768,2048]{1,0:T(8,128)(2,1)} %bitcast.190, bf16[768,512]{1,0:T(8,128)(2,1)S(1)} %get-tuple-element.32), kind=kOutput, calls=%fused_computation.225 | convolution fusion | flops 1610612736 | bytes 8126464 | tf_op jit(solution)/shard_map/dot_general | solution.py:27
  155.1 3.8 %fusion.132 = f32[2048,512]{1,0:T(8,128)} fusion(bf16[768,2048]{1,0:T(8,128)(2,1)S(1)} %bitcast.192, bf16[768,512]{1,0:T(8,128)(2,1)S(1)} %copy-done.4), kind=kOutput, calls=%fused_computation.226 | convolution fusion | flops 1610612736 | bytes 8126464 | tf_op jit(solution)/shard_map/dot_general | solution.py:27
  159.0 4.0 %fusion.48 = f32[512,2048]{1,0:T(8,128)} fusion(bf16[768,2048]{1,0:T(8,128)(2,1)S(1)} %bitcast.194, f32[768,512]{1,0:T(8,128)S(1)} %copy-done.17, f32[768,512]{1,0:T(8,128)S(1)} %copy-done.16), kind=kOutput, calls=%fused_computation.89 | convolution fusion | flops 1612972032 | bytes 10485760 | tf_op jit(solution)/shard_map/dot_general | solution.py:27
  163.0 18.7 %all-to-all-done.2 = bf16[16,48,1024]{2,1,0:T(8,128)(2,1)} async-done(((bf16[16,48,1024]{2,1,0:T(8,128)(2,1)}), bf16[16,48,1024]{2,1,0:T(8,128)(2,1)}, u32[]{:S(2)}, u32[]{:S(2)}) %all-to-all-start.2) | async-done | bytes 1572896 | tf_op jit(solution)/shard_map/all_to_all | solution.py:310
  181.7 1.9 fusion.7
  183.7 1.7 collective-permute-done.1
  185.8 1.0 pad_maximum_fusion.2
  186.7 4.5 %all-to-all-start.3 = ((bf16[4,192,512]{2,1,0:T(8,128)(2,1)}), bf16[4,192,512]{2,1,0:T(8,128)(2,1)S(1)}, u32[]{:S(2)}, u32[]{:S(2)}) async-start(bf16[4,192,512]{2,1,0:T(8,128)(2,1)} %pad_maximum_fusion.2), calls=%async_computation.3 | async-start | bytes 1572864 | tf_op jit(solution)/shard_map/all_to_all | solution.py:339
  191.2 0.9 pad_maximum_fusion.3.mid_ref
  192.1 6.9 %shard_map.162 = (bf16[192,1024]{1,0:T(8,128)(2,1)}, f32[192,1024]{1,0:T(8,128)}, f32[192,1024]{1,0:T(8,128)}, f32[2,1024]{1,0:T(2,128)}) custom-call(bf16[192,2048]{1,0:T(8,128)(2,1)} %pad_maximum_fusion.3.mid_ref, bf16[1024,2048]{1,0:T(8,128)(2,1)} %w_ref.1, bf16[192,1024]{1,0:T(8,128)(2,1)} %pre_ref.1, bf16[192,1024]{1,0:T(8,128)(2,1)} %prev_ref.1, ...), custom_call_target="tpu_custom_call" | custom-call | flops 805306368 | bytes 8388608 | tf_op jit(solution)/shard_map/pallas_call | solution.py:80
  199.0 3.4 %all-to-all-done.3 = bf16[4,192,512]{2,1,0:T(8,128)(2,1)S(1)} async-done(((bf16[4,192,512]{2,1,0:T(8,128)(2,1)}), bf16[4,192,512]{2,1,0:T(8,128)(2,1)S(1)}, u32[]{:S(2)}, u32[]{:S(2)}) %all-to-all-start.3) | async-done | bytes 786464 | tf_op jit(solution)/shard_map/all_to_all | solution.py:339
  202.4 3.4 %convolution_convert_fusion = bf16[512,1024]{1,0:T(8,128)(2,1)} fusion(bf16[768,512]{1,0:T(8,128)(2,1)S(1)} %bitcast.129, bf16[768,1024]{1,0:T(8,128)(2,1)} %all-gather.15.cloned.1.call-done), kind=kOutput, calls=%fused_computation.16 | convolution fusion | flops 805830656 | bytes 3407872 | tf_op jit(solution)/shard_map/dot_general | solution.py:27
  205.8 0.7 slice.171
  206.5 3.3 %collective-permute-start.2 = (bf16[1,1024]{1,0:T(2,128)(2,1)S(1)}, bf16[1,1024]{1,0:T(2,128)(2,1)S(1)}, u32[]{:S(2)}, u32[]{:S(2)}) collective-permute-start(bf16[1,1024]{1,0:T(2,128)(2,1)S(1)} %slice.171), channel_id=1, source_target_pairs={{0,2},{2,4},{4,6},{6,8},{8,10},{10,12},{12,14},{14,16},{16,18},{18... | collective-permute-start | bytes 6152 | tf_op jit(solution)/shard_map/ppermute | solution.py:19
  209.9 12.4 %shard_map.163.edges_ref = f32[16,2,1024]{2,1,0:T(2,128)} custom-call(f32[2,1024]{1,0:T(2,128)} %get-tuple-element.26.edge_ref), custom_call_target="tpu_custom_call" | custom-call | bytes 16777216 | tf_op jit(solution)/shard_map/pallas_call | solution.py:172
  222.3 0.6 copy-done.10
  222.9 4.0 %shard_map.164 = (f32[192,1024]{1,0:T(8,128)}, f32[192,1024]{1,0:T(8,128)}) custom-call(s32[1]{0:T(128)} %bitcast.78.mine_ref, f32[16,2,1024]{2,1,0:T(2,128)} %shard_map.163.edges_ref, f32[192,1024]{1,0:T(8,128)} %get-tuple-element.27.grad_ref, f32[192,1024]{1,0:T(8,128)} %get-tuple-element.28.coef_ref, f32[192,1024]{1,0:T(8,128)} %log_ref.3, ...), custom_call_target="tpu_custom_call" | custom-call | flops 1572864 | bytes 5242880 | tf_op jit(solution)/shard_map/pallas_call | solution.py:122
  226.9 10.2 %reduce-scatter.2.cloned.1.call-done = bf16[128,1024]{1,0:T(8,128)(2,1)} async-done(((bf16[512,1024]{1,0:T(8,128)(2,1)}), bf16[128,1024]{1,0:T(8,128)(2,1)}) %reduce-scatter.2.cloned.1.call-update) | async-done | bytes 262160 | tf_op jit(solution)/shard_map/reduce_scatter | solution.py:346
  237.1 1.8 convert_element_type.429
  (90 shorter events, 2.4 us)
Async XLA Ops:
  8.0 107.1 %copy-start = (bf16[1,2048,512]{2,1,0:T(8,128)(2,1)S(1)}, bf16[1,2048,512]{2,1,0:T(8,128)(2,1)}, u32[]{:S(2)}) copy-start(bf16[1,2048,512]{2,1,0:T(8,128)(2,1)} %param.19) | copy-start | bytes 6291460
  8.0 3.9 %copy-start.9 = (s32[192,2]{0,1:T(2,128)S(1)}, s32[192,2]{0,1:T(2,128)}, u32[]{:S(2)}) copy-start(s32[192,2]{0,1:T(2,128)} %param.13) | copy-start | bytes 4612
  8.0 3.9 %copy-start.11 = (f32[192,2]{0,1:T(2,128)S(1)}, f32[192,2]{0,1:T(2,128)}, u32[]{:S(2)}) copy-start(f32[192,2]{0,1:T(2,128)} %param.14) | copy-start | bytes 4612
  8.0 42.8 %all-gather.11.cloned.1.call-start = ((), (), s32[]{:S(2)}) async-start(), calls=%async_computation.7 | async-start | bytes 1966080 | tf_op jit(solution)/shard_map/all_gather | solution.py:234
  10.0 78.9 %all-gather.7.cloned.1.call-start = ((), (), s32[]{:S(2)}) async-start(), calls=%async_computation.5 | async-start | bytes 1966080 | tf_op jit(solution)/shard_map/all_gather | solution.py:234
  50.8 2.9 %copy-start.15 = (bf16[768,1024]{1,0:T(8,128)(2,1)S(1)}, bf16[768,1024]{1,0:T(8,128)(2,1)}, u32[]{:S(2)}) copy-start(bf16[768,1024]{1,0:T(8,128)(2,1)} %all-gather.11.cloned.1.call-done) | copy-start | bytes 4718596
  55.9 23.1 %all-to-all-start.1 = ((bf16[4,192,1024]{2,1,0:T(8,128)(2,1)}), bf16[4,192,1024]{2,1,0:T(8,128)(2,1)}, u32[]{:S(2)}, u32[]{:S(2)}) async-start(bf16[4,192,1024]{2,1,0:T(8,128)(2,1)} %bitcast.126), calls=%async_computation.1 | async-start | bytes 3145728 | tf_op jit(solution)/shard_map/all_to_all | solution.py:272
  60.3 54.8 %all-gather.13.cloned.1.call-start = ((), (), s32[]{:S(2)}) async-start(), calls=%async_computation.8 | async-start | bytes 4718592 | tf_op jit(solution)/shard_map/all_gather | solution.py:278
  79.0 46.8 %all-gather.9.cloned.1.call-start = ((), (), s32[]{:S(2)}) async-start(), calls=%async_computation.6 | async-start | bytes 4718592 | tf_op jit(solution)/shard_map/all_gather | solution.py:279
  115.1 5.0 %copy-start.5 = (bf16[1,2048,512]{2,1,0:T(8,128)(2,1)S(1)}, bf16[1,2048,512]{2,1,0:T(8,128)(2,1)}, u32[]{:S(2)}) copy-start(bf16[1,2048,512]{2,1,0:T(8,128)(2,1)} %param.20) | copy-start | bytes 6291460
  115.1 5.0 %copy-start.12 = (bf16[4,192,2048]{2,1,0:T(8,128)(2,1)S(1)}, bf16[4,192,2048]{2,1,0:T(8,128)(2,1)}, u32[]{:S(2)}) copy-start(bf16[4,192,2048]{2,1,0:T(8,128)(2,1)} %all-gather.13.cloned.1.call-done) | copy-start | bytes 9437188
  131.5 6.4 %copy-start.3 = (bf16[768,512]{1,0:T(8,128)(2,1)}, bf16[768,512]{1,0:T(8,128)(2,1)S(1)}, u32[]{:S(2)}) copy-start(bf16[768,512]{1,0:T(8,128)(2,1)S(1)} %get-tuple-element.31) | copy-start | bytes 2359300
  131.5 1.9 copy-start.6
  134.4 3.5 %collective-permute-start = (bf16[768,1024]{1,0:T(8,128)(2,1)S(1)}, bf16[768,1024]{1,0:T(8,128)(2,1)S(1)}, u32[]{:S(2)}, u32[]{:S(2)}) collective-permute-start(bf16[768,1024]{1,0:T(8,128)(2,1)S(1)} %add_convert_fusion.1), channel_id=1, source_target_pairs={{0,1},{1,0},{2,3},{3,2},{4,5},{5,4},{6,7},{7,6},{8,9},{9,8},{10,11... | collective-permute-start | bytes 4718600 | tf_op jit(solution)/shard_map/ppermute | solution.py:23
  140.2 7.3 %copy-start.2 = (bf16[192,1024]{1,0:T(8,128)(2,1)S(1)}, bf16[192,1024]{1,0:T(8,128)(2,1)}, u32[]{:S(2)}) copy-start(bf16[192,1024]{1,0:T(8,128)(2,1)} %prev_ref.1) | copy-start | bytes 1179652
  140.2 7.3 %copy-start.7 = (bf16[192,1024]{1,0:T(8,128)(2,1)S(1)}, bf16[192,1024]{1,0:T(8,128)(2,1)}, u32[]{:S(2)}) copy-start(bf16[192,1024]{1,0:T(8,128)(2,1)} %pre_ref.1) | copy-start | bytes 1179652
  140.3 41.4 %all-to-all-start.2 = ((bf16[16,48,1024]{2,1,0:T(8,128)(2,1)}), bf16[16,48,1024]{2,1,0:T(8,128)(2,1)}, u32[]{:S(2)}, u32[]{:S(2)}) async-start(bf16[16,48,1024]{2,1,0:T(8,128)(2,1)} %bitcast.62), calls=%async_computation.2 | async-start | bytes 3145728 | tf_op jit(solution)/shard_map/all_to_all | solution.py:310
  147.2 55.2 %all-gather.15.cloned.1.call-start = ((), (), s32[]{:S(2)}) async-start(), calls=%async_computation.9 | async-start | bytes 1966080 | tf_op jit(solution)/shard_map/all_gather | solution.py:283
  149.2 5.9 %copy-start.4 = (bf16[768,512]{1,0:T(8,128)(2,1)S(1)}, bf16[768,512]{1,0:T(8,128)(2,1)}, u32[]{:S(2)}) copy-start(bf16[768,512]{1,0:T(8,128)(2,1)} %copy-done.3) | copy-start | bytes 2359300
  149.2 5.9 %copy-start.13 = (bf16[4,192,2048]{2,1,0:T(8,128)(2,1)S(1)}, bf16[4,192,2048]{2,1,0:T(8,128)(2,1)}, u32[]{:S(2)}) copy-start(bf16[4,192,2048]{2,1,0:T(8,128)(2,1)} %all-gather.13.cloned.1.call-done) | copy-start | bytes 9437188
  155.1 3.9 %copy-start.14 = (bf16[4,192,2048]{2,1,0:T(8,128)(2,1)S(1)}, bf16[4,192,2048]{2,1,0:T(8,128)(2,1)}, u32[]{:S(2)}) copy-start(bf16[4,192,2048]{2,1,0:T(8,128)(2,1)} %all-gather.9.cloned.1.call-done) | copy-start | bytes 9437188
  155.1 3.9 %copy-start.16 = (f32[768,512]{1,0:T(8,128)S(1)}, f32[768,512]{1,0:T(8,128)}, u32[]{:S(2)}) copy-start(f32[768,512]{1,0:T(8,128)} %fusion) | copy-start | bytes 4718596
  155.1 3.9 %copy-start.17 = (f32[768,512]{1,0:T(8,128)S(1)}, f32[768,512]{1,0:T(8,128)}, u32[]{:S(2)}) copy-start(f32[768,512]{1,0:T(8,128)} %fusion.2) | copy-start | bytes 4718596
  159.0 22.7 %copy-start.8 = (bf16[192,1024]{1,0:T(8,128)(2,1)S(1)}, bf16[192,1024]{1,0:T(8,128)(2,1)}, u32[]{:S(2)}) copy-start(bf16[192,1024]{1,0:T(8,128)(2,1)} %constant_dynamic-slice_fusion.1) | copy-start | bytes 1179652
  183.6 1.8 collective-permute-start.1
  186.7 15.7 %all-to-all-start.3 = ((bf16[4,192,512]{2,1,0:T(8,128)(2,1)}), bf16[4,192,512]{2,1,0:T(8,128)(2,1)S(1)}, u32[]{:S(2)}, u32[]{:S(2)}) async-start(bf16[4,192,512]{2,1,0:T(8,128)(2,1)} %pad_maximum_fusion.2), calls=%async_computation.3 | async-start | bytes 1572864 | tf_op jit(solution)/shard_map/all_to_all | solution.py:339
  191.2 45.9 %reduce-scatter.2.cloned.1.call-start = ((), (), s32[]{:S(2)}) async-start(), calls=%async_computation.10 | async-start | bytes 1310720 | tf_op jit(solution)/shard_map/reduce_scatter | solution.py:346
  206.5 15.7 %collective-permute-start.2 = (bf16[1,1024]{1,0:T(2,128)(2,1)S(1)}, bf16[1,1024]{1,0:T(2,128)(2,1)S(1)}, u32[]{:S(2)}, u32[]{:S(2)}) collective-permute-start(bf16[1,1024]{1,0:T(2,128)(2,1)S(1)} %slice.171), channel_id=1, source_target_pairs={{0,2},{2,4},{4,6},{6,8},{8,10},{10,12},{12,14},{14,16},{16,18},{18... | collective-permute-start | bytes 6152 | tf_op jit(solution)/shard_map/ppermute | solution.py:19
  222.3 0.6 copy-start.10
  222.3 16.6 %copy-start.1 = (bf16[1,2048,512]{2,1,0:T(8,128)(2,1)S(1)}, bf16[1,2048,512]{2,1,0:T(8,128)(2,1)}, u32[]{:S(2)}) copy-start(bf16[1,2048,512]{2,1,0:T(8,128)(2,1)} %param.19) | copy-start | bytes 6291460
Sparse Core Ops, SparseCore 0:
  11.0 39.7 all-gather.10
  53.0 35.8 all-gather.6
  90.4 10.9 all-gather.12
  115.2 10.5 all-gather.8
  205.9 31.0 reduce-scatter.1
Sparse Core Ops, SparseCore 1:
  149.5 40.3 all-gather.14
